TPU v7x, 32 devices: a whole 2x2x4 slice. The times are simulated.
32 devices in a mesh: sp: 8 (over z, x), tp: 4 (over y, core).
Axes of the slice: x: 2, y: 2, z: 4, core: 2. Of those that a mesh axis runs over, the one named last changes fastest.
Arguments:
- out_grad: bfloat16 [1024, 2048], P('sp', 'tp'), may hold values from -6 to 6
- moe_input: bfloat16 [1024, 2048], P('sp', 'tp'), may hold values from -6 to 6
- route_weight: float32 [1024, 2], P('sp'), may hold values from 0.2 to 1
- route_ids: int32 [1024, 2], P('sp'), may hold values from 0 to 7, all different within a row; in each aligned block of 128 rows (0 to 127, 128 to 255, ...) at most 64 rows name the same one
- gate_proj: bfloat16 [8, 2048, 2816], P('sp', None, 'tp'), may hold values from -0.125 to 0.125
- up_proj: bfloat16 [8, 2048, 2816], P('sp', None, 'tp'), may hold values from -0.125 to 0.125
- down_proj: bfloat16 [8, 2816, 2048], P('sp', 'tp'), may hold values from -0.109375 to 0.109375
- out_proj: bfloat16 [2048, 2048], P(None, 'tp'), may hold values from -0.125 to 0.125
- conv_out: bfloat16 [1024, 2048], P('sp', 'tp'), may hold values from -6 to 6
- gate_b: bfloat16 [1024, 2048], P('sp', 'tp'), may hold values from -6 to 6
- gate_c: bfloat16 [1024, 2048], P('sp', 'tp'), may hold values from -6 to 6
- value_v: bfloat16 [1024, 2048], P('sp', 'tp'), may hold values from -6 to 6
- conv_taps: float32 [3, 2048], P(None, 'tp'), may hold values from -3 to 3
Outputs:
- grad_gate: bfloat16 [8, 2048, 2816], P('sp', None, 'tp')
- grad_up: bfloat16 [8, 2048, 2816], P('sp', None, 'tp')
- grad_down: bfloat16 [8, 2816, 2048], P('sp', 'tp')
- grad_out: float32 [2048, 2048], P('sp', 'tp')
- grad_b: bfloat16 [1024, 2048], P('sp', 'tp')
- grad_c: bfloat16 [1024, 2048], P('sp', 'tp')
- grad_v: bfloat16 [1024, 2048], P('sp', 'tp')
Inputs may be any that keep to these rules, and one draw needn't show every extreme that they name: `route_ids`: each row names two different experts; within the 128 rows of one index of sp no expert is named by more than 64 rows, a bound that some block reaches.
All inputs are finite; a program needn't handle non-finite values.
Results may differ from a plain program's by a relative error of at most 0.019.
Values may be sent and summed in bfloat16 or wider, within the bound.
A program may use at most 64 MiB of HBM per device.

v0:
```python
import jax
import jax.numpy as jnp
from jax import lax
from jax.sharding import PartitionSpec as P


def with_halo(block, sides, width):
    for axis, dim in sides:
        count = lax.axis_size(axis)
        forward = [(i, i + 1) for i in range(count - 1)]
        backward = [(target, source) for source, target in forward]
        low = lax.ppermute(
            lax.slice_in_dim(block, block.shape[dim] - width, None, axis=dim), axis, forward
        )
        high = lax.ppermute(lax.slice_in_dim(block, 0, width, axis=dim), axis, backward)
        block = jnp.concatenate([low, block, high], axis=dim)
    return block


def place_rows(rows, index, total):
    return jnp.zeros((total, rows.shape[1]), rows.dtype).at[index].set(rows)


def local(
    out_grad,
    moe_input,
    route_weight,
    route_ids,
    gate_proj,
    up_proj,
    down_proj,
    out_proj,
    conv_out,
    gate_b,
    gate_c,
    value_v,
    conv_taps,
):
    tok_rows = out_grad.shape[0]
    local_cols = out_grad.shape[1]
    n_experts = lax.axis_size("sp")
    capacity = 4 * tok_rows // n_experts
    flat = route_ids.reshape(2 * tok_rows)
    onehot = (flat[:, None] == jnp.arange(n_experts, dtype=jnp.int32)[None, :]).astype(jnp.int32)
    before = jnp.cumsum(onehot, axis=0) - onehot
    slot = jnp.sum(before * onehot, axis=1)
    dest = flat * capacity + slot
    total = n_experts * capacity
    rows_x = jnp.broadcast_to(moe_input[:, None, :], (tok_rows, 2, local_cols)).reshape(
        2 * tok_rows, local_cols
    )
    rows_dy = (
        (route_weight[:, :, None] * out_grad.astype(jnp.float32)[:, None, :])
        .astype(jnp.bfloat16)
        .reshape(2 * tok_rows, local_cols)
    )
    send_x = place_rows(rows_x, dest, total).reshape(n_experts, capacity, local_cols)
    send_dy = place_rows(rows_dy, dest, total).reshape(n_experts, capacity, local_cols)
    part_x, part_dy = (
        lax.all_to_all(send_x, "sp", split_axis=0, concat_axis=0, tiled=True),
        lax.all_to_all(send_dy, "sp", split_axis=0, concat_axis=0, tiled=True),
    )
    recv_x, recv_dy = (
        lax.all_gather(part_x, "tp", axis=2, tiled=True),
        lax.all_gather(part_dy, "tp", axis=2, tiled=True),
    )
    width = recv_x.shape[2]
    xin = recv_x.reshape(total, width)
    dyin = recv_dy.reshape(total, width)
    w_gate = gate_proj[0]
    w_up = up_proj[0]
    w_down = down_proj[0]
    gate = jnp.dot(xin, w_gate, preferred_element_type=jnp.float32)
    upval = jnp.dot(xin, w_up, preferred_element_type=jnp.float32)
    sig = jax.nn.sigmoid(gate)
    act = gate * sig
    hidden = (act * upval).astype(jnp.bfloat16)
    grad_down = jnp.dot(hidden.T, dyin, preferred_element_type=jnp.float32).astype(jnp.bfloat16)
    dhid = jnp.dot(dyin, w_down.T, preferred_element_type=jnp.float32)
    dgate = (dhid * upval * (sig * (1.0 + gate * (1.0 - sig)))).astype(jnp.bfloat16)
    dup = (dhid * act).astype(jnp.bfloat16)
    grad_gate = jnp.dot(xin.T, dgate, preferred_element_type=jnp.float32).astype(jnp.bfloat16)
    grad_up = jnp.dot(xin.T, dup, preferred_element_type=jnp.float32).astype(jnp.bfloat16)
    partial_value = jnp.dot(dgate, w_gate.T, preferred_element_type=jnp.float32) + jnp.dot(
        dup, w_up.T, preferred_element_type=jnp.float32
    )
    partial_value = lax.optimization_barrier(partial_value.astype(jnp.bfloat16)).astype(jnp.float32)
    summed = lax.psum_scatter(
        partial_value.astype(jnp.bfloat16), "tp", scatter_dimension=1, tiled=True
    )
    returned = lax.all_to_all(
        summed.reshape(n_experts, capacity, local_cols),
        "sp",
        split_axis=0,
        concat_axis=0,
        tiled=True,
    )
    picked = returned.reshape(total, local_cols)[dest]
    moe_grad = jnp.sum(picked.reshape(tok_rows, 2, local_cols).astype(jnp.float32), axis=1)
    grad_h = (out_grad.astype(jnp.float32) + moe_grad).astype(jnp.bfloat16)
    full_h = lax.all_gather(grad_h, "tp", axis=1, tiled=True)
    grad_z = jnp.dot(full_h, out_proj, preferred_element_type=jnp.float32)
    dconv = (grad_z * gate_b.astype(jnp.float32)).astype(jnp.bfloat16)
    grad_b = (grad_z * conv_out.astype(jnp.float32)).astype(jnp.bfloat16)
    padded = with_halo(dconv, (("sp", 0),), 1).astype(jnp.float32)
    grad_u = conv_taps[0] * padded[2:] + conv_taps[1] * padded[1:-1] + conv_taps[2] * padded[:-2]
    grad_c = (grad_u * value_v.astype(jnp.float32)).astype(jnp.bfloat16)
    grad_v = (grad_u * gate_c.astype(jnp.float32)).astype(jnp.bfloat16)
    mixed = (gate_b.astype(jnp.float32) * conv_out.astype(jnp.float32)).astype(jnp.bfloat16)
    grad_out = lax.psum_scatter(
        lax.dot_general(
            full_h, mixed, (((0,), (0,)), ((), ())), preferred_element_type=jnp.float32
        ).astype(jnp.bfloat16),
        "sp",
        scatter_dimension=0,
        tiled=True,
    ).astype(jnp.float32)
    return (grad_gate[None], grad_up[None], grad_down[None], grad_out, grad_b, grad_c, grad_v)


def solution(mesh):
    in_specs = (
        P("sp", "tp"),
        P("sp", "tp"),
        P("sp", None),
        P("sp", None),
        P("sp", None, "tp"),
        P("sp", None, "tp"),
        P("sp", "tp", None),
        P(None, "tp"),
        P("sp", "tp"),
        P("sp", "tp"),
        P("sp", "tp"),
        P("sp", "tp"),
        P(None, "tp"),
    )
    out_specs = (
        P("sp", None, "tp"),
        P("sp", None, "tp"),
        P("sp", "tp", None),
        P("sp", "tp"),
        P("sp", "tp"),
        P("sp", "tp"),
        P("sp", "tp"),
    )
    return jax.shard_map(local, mesh=mesh, in_specs=in_specs, out_specs=out_specs, check_vma=False)
```

profile of v0, /device:TPU:0, one launch (start us, length us, event | category | flops | bytes accessed | tf_op | source)
XLA Modules:
  0.0 235.1 jit_solution(585506620943027061)
XLA Ops:
  7.2 0.0 copy-start
  7.2 0.0 copy-start.6
  7.2 0.0 all-gather.3.cloned.1.call-start
  7.2 0.9 copy.21
  8.2 0.1 eq.29
  8.3 0.1 eq.25
  8.5 0.7 broadcast_multiply_fusion
  9.2 0.6 reduce-window.6
  9.7 0.2 slice_reduce_fusion
  10.0 0.1 copy.20
  10.1 0.1 mul.105
  10.2 1.0 broadcast_in_dim.8
  11.3 0.0 copy-start.10
  11.3 0.8 reshape.112
  12.1 0.1 fusion.26
  12.2 2.1 scatter_custom_fusion
  14.3 21.7 %all_to_all.15 = bf16[8,64,512]{2,1,0:T(8,128)(2,1)} all-to-all(bf16[8,64,512]{2,1,0:T(8,128)(2,1)S(1)} %bitcast.55), channel_id=1, replica_groups=mesh['sp'=8,'tp'=4] {'sp'}, dimensions={0} | all-to-all | bytes 1048576 | tf_op jit(solution)/shard_map/all_to_all | solution.py:60
  36.0 0.0 all-gather.3.cloned.1.call-update
  36.0 0.0 all-gather.5.cloned.1.call-start
  36.1 0.1 mul.109
  36.2 1.2 mul.110
  37.4 0.1 copy.23
  37.5 0.1 mul.107
  37.6 2.2 scatter_custom_fusion.1
  39.9 17.6 %all_to_all.16 = bf16[8,64,512]{2,1,0:T(8,128)(2,1)} all-to-all(bf16[8,64,512]{2,1,0:T(8,128)(2,1)S(1)} %bitcast.54), channel_id=1, replica_groups=mesh['sp'=8,'tp'=4] {'sp'}, dimensions={0} | all-to-all | bytes 1048576 | tf_op jit(solution)/shard_map/all_to_all | solution.py:61
  57.5 0.0 all-gather.5.cloned.1.call-update
  57.5 0.2 reduce-scatter.3.cloned.1.call-start
  57.8 0.0 all-gather.3.cloned.1.call-done
  57.8 0.0 copy-start.11
  57.8 4.5 %fusion.5 = f32[512,704]{0,1:T(8,128)} fusion(bf16[512,2048]{1,0:T(8,128)(2,1)} %bitcast.64, bf16[1,2048,704]{1,2,0:T(8,128)(2,1)S(1)} %copy-done), kind=kOutput, calls=%fused_computation.13 | convolution fusion | flops 1476395008 | bytes 6422528 | tf_op jit(solution)/shard_map/dot_general | solution.py:73
  62.4 2.8 %fusion.8 = f32[512,704]{0,1:T(8,128)} fusion(bf16[512,2048]{1,0:T(8,128)(2,1)S(1)} %bitcast.66, bf16[1,2048,704]{1,2,0:T(8,128)(2,1)S(1)} %copy-done.11), kind=kOutput, calls=%fused_computation.16 | convolution fusion | flops 1476395008 | bytes 6422528 | tf_op jit(solution)/shard_map/dot_general | solution.py:74
  65.1 16.8 %all-gather.5.cloned.1.call-done = bf16[8,64,2048]{2,1,0:T(8,128)(2,1)} async-done(((bf16[8,64,512]{2,1,0:T(8,128)(2,1)}), bf16[8,64,2048]{2,1,0:T(8,128)(2,1)}) %all-gather.5.cloned.1.call-update) | async-done | bytes 2097168 | tf_op jit(solution)/shard_map/all_gather | solution.py:65
  81.9 5.4 %multiply_convert_fusion.1 = (bf16[512,704]{0,1:T(8,128)(2,1)S(1)}, bf16[512,704]{0,1:T(8,128)(2,1)S(1)}) fusion(f32[512,704]{0,1:T(8,128)} %fusion.5, f32[512,704]{0,1:T(8,128)} %fusion.8, bf16[512,2048]{1,0:T(8,128)(2,1)} %bitcast.68, bf16[1,704,2048]{2,1,0:T(8,128)(2,1)} %param.19), kind=kOutput, calls=%fused_computation.21 | convolution fusion | flops 1481080832 | bytes 9306112 | tf_op jit(solution)/shard_map/dot_general | solution.py:79
  87.3 0.0 copy-start.12
  87.3 1.9 fusion.3
  89.3 0.4 copy-done.12
  89.7 3.3 %add_convert_fusion = bf16[512,2048]{1,0:T(8,128)(2,1)} fusion(f32[512,2048]{1,0:T(8,128)S(1)} %fusion.3, bf16[512,704]{0,1:T(8,128)(2,1)S(1)} %get-tuple-element.9, bf16[1,2048,704]{1,2,0:T(8,128)(2,1)S(1)} %copy-done.12), kind=kOutput, calls=%fused_computation.3 | convolution fusion | flops 1478492160 | bytes 9895936 | tf_op jit(solution)/shard_map/dot_general | solution.py:84
  93.0 0.0 reduce-scatter.3.cloned.1.call-update
  93.0 31.3 %reduce-scatter.3.cloned.1.call-done = bf16[512,512]{1,0:T(8,128)(2,1)} async-done(((bf16[512,2048]{1,0:T(8,128)(2,1)}), bf16[512,512]{1,0:T(8,128)(2,1)}) %reduce-scatter.3.cloned.1.call-update) | async-done | bytes 524304 | tf_op jit(solution)/shard_map/reduce_scatter | solution.py:88
  124.3 5.5 %all-to-all-start.2 = ((bf16[8,64,512]{2,1,0:T(8,128)(2,1)}), bf16[8,64,512]{2,1,0:T(8,128)(2,1)S(1)}, u32[]{:S(2)}, u32[]{:S(2)}) async-start(bf16[8,64,512]{2,1,0:T(8,128)(2,1)} %bitcast.56), calls=%async_computation.3 | async-start | bytes 1048576 | tf_op jit(solution)/shard_map/all_to_all | solution.py:91
  129.9 0.0 reduce-scatter.5.cloned.1.call-start
  129.9 14.3 %all-to-all-done.2 = bf16[8,64,512]{2,1,0:T(8,128)(2,1)S(1)} async-done(((bf16[8,64,512]{2,1,0:T(8,128)(2,1)}), bf16[8,64,512]{2,1,0:T(8,128)(2,1)S(1)}, u32[]{:S(2)}, u32[]{:S(2)}) %all-to-all-start.2) | async-done | bytes 524320 | tf_op jit(solution)/shard_map/all_to_all | solution.py:91
  144.2 1.9 gather_fusion
  146.0 1.3 reshape.99
  147.3 1.3 reduce_sum.22
  148.7 1.0 add_convert_fusion.1
  149.7 6.7 %all_gather.11 = bf16[128,2048]{1,0:T(8,128)(2,1)S(1)} all-gather(bf16[128,512]{1,0:T(8,128)(2,1)S(1)} %add_convert_fusion.1), channel_id=1, replica_groups=mesh['sp'=8,'tp'=4] {'tp'}, dimensions={1}, use_global_device_ids=true | all-gather | bytes 655360 | tf_op jit(solution)/shard_map/all_gather | solution.py:101
  156.4 3.0 %convolution_convert_fusion.3 = bf16[2048,512]{1,0:T(8,128)(2,1)} fusion(bf16[128,2048]{1,0:T(8,128)(2,1)S(1)} %all_gather.11, bf16[128,512]{1,0:T(8,128)(2,1)S(1)} %copy-done.4, bf16[128,512]{1,0:T(8,128)(2,1)} %param.22), kind=kOutput, calls=%fused_computation.7 | convolution fusion | flops 269746176 | bytes 2883584 | tf_op jit(solution)/shard_map/dot_general | solution.py:111
  159.4 0.0 reduce-scatter.5.cloned.1.call-update
  159.5 5.2 %fusion.2 = bf16[1,2048,704]{1,2,0:T(8,128)(2,1)} fusion(bf16[512,704]{0,1:T(8,128)(2,1)} %copy-done.16, bf16[512,2048]{1,0:T(8,128)(2,1)} %bitcast.65), kind=kOutput, calls=%fused_computation.10 | convolution fusion | flops 1477836800 | bytes 5701632 | tf_op jit(solution)/shard_map/dot_general | solution.py:83
  164.7 0.0 copy-start.1
  164.7 0.0 copy-start.5
  164.7 3.3 %fusion = bf16[1,704,2048]{2,1,0:T(8,128)(2,1)} fusion(bf16[512,2048]{1,0:T(8,128)(2,1)S(1)} %bitcast.69, f32[512,704]{0,1:T(8,128)S(1)} %copy-done.18, f32[512,704]{0,1:T(8,128)S(1)} %copy-done.17), kind=kOutput, calls=%fused_computation.8 | convolution fusion | flops 1479999488 | bytes 7864320 | tf_op jit(solution)/shard_map/dot_general | solution.py:78
  168.0 1.1 fusion.13
  169.2 3.4 %collective-permute-start = (bf16[1,512]{1,0:T(2,128)(2,1)S(1)}, bf16[1,512]{1,0:T(2,128)(2,1)S(1)}, u32[]{:S(2)}, u32[]{:S(2)}) collective-permute-start(bf16[1,512]{1,0:T(2,128)(2,1)S(1)} %get-tuple-element.13), channel_id=1, source_target_pairs={{0,4},{4,8},{8,12},{12,16},{16,20},{20,24},{24,28},{1,5},{5,9},{9,... | collective-permute-start | bytes 3080 | tf_op jit(solution)/shard_map/ppermute | solution.py:12
  172.5 0.0 copy-start.7
  172.6 0.0 copy-start.8
  172.6 1.4 collective-permute-start.1
  174.0 3.2 %fusion.1 = bf16[1,2048,704]{1,2,0:T(8,128)(2,1)} fusion(bf16[512,704]{0,1:T(8,128)(2,1)S(1)} %copy-done.3, bf16[512,2048]{1,0:T(8,128)(2,1)S(1)} %bitcast.67), kind=kOutput, calls=%fused_computation.9 | convolution fusion | flops 1477836800 | bytes 5701632 | tf_op jit(solution)/shard_map/dot_general | solution.py:82
  177.3 0.9 collective-permute-done.1
  178.2 0.8 multiply_convert_fusion.6
  179.0 0.7 multiply_convert_fusion.7
  179.7 47.0 %reduce-scatter.5.cloned.1.call-done = bf16[256,512]{1,0:T(8,128)(2,1)} async-done(((bf16[2048,512]{1,0:T(8,128)(2,1)}), bf16[256,512]{1,0:T(8,128)(2,1)}) %reduce-scatter.5.cloned.1.call-update) | async-done | bytes 262160 | tf_op jit(solution)/shard_map/reduce_scatter | solution.py:110
  226.7 1.8 convert_element_type.103
  (37 shorter events, 0.2 us)
Async XLA Ops:
  7.2 50.6 %copy-start = (bf16[1,2048,704]{1,2,0:T(8,128)(2,1)S(1)}, bf16[1,2048,704]{1,2,0:T(8,128)(2,1)}, u32[]{:S(2)}) copy-start(bf16[1,2048,704]{1,2,0:T(8,128)(2,1)} %param.17) | copy-start | bytes 8650756
  7.2 28.9 %copy-start.6 = (bf16[128,512]{1,0:T(8,128)(2,1)S(1)}, bf16[128,512]{1,0:T(8,128)(2,1)}, u32[]{:S(2)}) copy-start(bf16[128,512]{1,0:T(8,128)(2,1)} %param.13) | copy-start | bytes 393220
  7.2 50.6 %all-gather.3.cloned.1.call-start = ((), (), s32[]{:S(2)}) async-start(), calls=%async_computation.5 | async-start | bytes 2621440 | tf_op jit(solution)/shard_map/all_gather | solution.py:64
  11.3 26.1 %copy-start.10 = (f32[128,2]{0,1:T(2,128)S(1)}, f32[128,2]{0,1:T(2,128)}, u32[]{:S(2)}) copy-start(f32[128,2]{0,1:T(2,128)} %param.15) | copy-start | bytes 3076
  36.0 45.9 %all-gather.5.cloned.1.call-start = ((), (), s32[]{:S(2)}) async-start(), calls=%async_computation.6 | async-start | bytes 2621440 | tf_op jit(solution)/shard_map/all_gather | solution.py:65
  57.5 66.8 %reduce-scatter.3.cloned.1.call-start = ((), (), s32[]{:S(2)}) async-start(), calls=%async_computation.7 | async-start | bytes 2621440 | tf_op jit(solution)/shard_map/reduce_scatter | solution.py:88
  57.8 4.6 %copy-start.11 = (bf16[1,2048,704]{1,2,0:T(8,128)(2,1)S(1)}, bf16[1,2048,704]{1,2,0:T(8,128)(2,1)}, u32[]{:S(2)}) copy-start(bf16[1,2048,704]{1,2,0:T(8,128)(2,1)} %param.18) | copy-start | bytes 8650756
  57.8 4.5 %copy-start.13 = (bf16[8,64,2048]{2,1,0:T(8,128)(2,1)S(1)}, bf16[8,64,2048]{2,1,0:T(8,128)(2,1)}, u32[]{:S(2)}) copy-start(bf16[8,64,2048]{2,1,0:T(8,128)(2,1)} %all-gather.3.cloned.1.call-done) | copy-start | bytes 6291460
  87.3 1.9 copy-start.2
  87.3 1.9 copy-start.16
  87.3 2.3 copy-start.12
  124.3 19.8 %all-to-all-start.2 = ((bf16[8,64,512]{2,1,0:T(8,128)(2,1)}), bf16[8,64,512]{2,1,0:T(8,128)(2,1)S(1)}, u32[]{:S(2)}, u32[]{:S(2)}) async-start(bf16[8,64,512]{2,1,0:T(8,128)(2,1)} %bitcast.56), calls=%async_computation.3 | async-start | bytes 1048576 | tf_op jit(solution)/shard_map/all_to_all | solution.py:91
  129.9 96.9 %reduce-scatter.5.cloned.1.call-start = ((), (), s32[]{:S(2)}) async-start(), calls=%async_computation.8 | async-start | bytes 2359296 | tf_op jit(solution)/shard_map/reduce_scatter | solution.py:110
  144.2 12.2 %copy-start.4 = (bf16[128,512]{1,0:T(8,128)(2,1)S(1)}, bf16[128,512]{1,0:T(8,128)(2,1)}, u32[]{:S(2)}) copy-start(bf16[128,512]{1,0:T(8,128)(2,1)} %param.21) | copy-start | bytes 393220
  156.4 3.0 %copy-start.9 = (f32[3,512]{1,0:T(4,128)S(1)}, f32[3,512]{1,0:T(4,128)}, u32[]{:S(2)}) copy-start(f32[3,512]{1,0:T(4,128)} %param.25) | copy-start | bytes 18436
  159.5 5.2 %copy-start.15 = (bf16[8,64,2048]{2,1,0:T(8,128)(2,1)S(1)}, bf16[8,64,2048]{2,1,0:T(8,128)(2,1)}, u32[]{:S(2)}) copy-start(bf16[8,64,2048]{2,1,0:T(8,128)(2,1)} %all-gather.5.cloned.1.call-done) | copy-start | bytes 6291460
  159.5 5.2 %copy-start.17 = (f32[512,704]{0,1:T(8,128)S(1)}, f32[512,704]{0,1:T(8,128)}, u32[]{:S(2)}) copy-start(f32[512,704]{0,1:T(8,128)} %fusion.5) | copy-start | bytes 4325380
  159.5 5.2 %copy-start.18 = (f32[512,704]{0,1:T(8,128)S(1)}, f32[512,704]{0,1:T(8,128)}, u32[]{:S(2)}) copy-start(f32[512,704]{0,1:T(8,128)} %fusion.8) | copy-start | bytes 4325380
  164.7 3.3 %copy-start.1 = (bf16[2048,512]{1,0:T(8,128)(2,1)S(1)}, bf16[2048,512]{1,0:T(8,128)(2,1)}, u32[]{:S(2)}) copy-start(bf16[2048,512]{1,0:T(8,128)(2,1)} %param.20) | copy-start | bytes 6291460
  164.7 3.3 %copy-start.5 = (bf16[128,512]{1,0:T(8,128)(2,1)S(1)}, bf16[128,512]{1,0:T(8,128)(2,1)}, u32[]{:S(2)}) copy-start(bf16[128,512]{1,0:T(8,128)(2,1)} %param.22) | copy-start | bytes 393220
  168.0 6.0 %copy-start.3 = (bf16[512,704]{0,1:T(8,128)(2,1)S(1)}, bf16[512,704]{0,1:T(8,128)(2,1)}, u32[]{:S(2)}) copy-start(bf16[512,704]{0,1:T(8,128)(2,1)} %copy-done.2) | copy-start | bytes 2162692
  168.0 6.0 %copy-start.14 = (bf16[8,64,2048]{2,1,0:T(8,128)(2,1)S(1)}, bf16[8,64,2048]{2,1,0:T(8,128)(2,1)}, u32[]{:S(2)}) copy-start(bf16[8,64,2048]{2,1,0:T(8,128)(2,1)} %all-gather.3.cloned.1.call-done) | copy-start | bytes 6291460
  169.2 8.1 %collective-permute-start = (bf16[1,512]{1,0:T(2,128)(2,1)S(1)}, bf16[1,512]{1,0:T(2,128)(2,1)S(1)}, u32[]{:S(2)}, u32[]{:S(2)}) collective-permute-start(bf16[1,512]{1,0:T(2,128)(2,1)S(1)} %get-tuple-element.13), channel_id=1, source_target_pairs={{0,4},{4,8},{8,12},{12,16},{16,20},{20,24},{24,28},{1,5},{5,9},{9,... | collective-permute-start | bytes 3080 | tf_op jit(solution)/shard_map/ppermute | solution.py:12
  172.5 5.7 %copy-start.7 = (bf16[128,512]{1,0:T(8,128)(2,1)S(1)}, bf16[128,512]{1,0:T(8,128)(2,1)}, u32[]{:S(2)}) copy-start(bf16[128,512]{1,0:T(8,128)(2,1)} %param.23) | copy-start | bytes 393220
  172.6 6.4 %copy-start.8 = (bf16[128,512]{1,0:T(8,128)(2,1)S(1)}, bf16[128,512]{1,0:T(8,128)(2,1)}, u32[]{:S(2)}) copy-start(bf16[128,512]{1,0:T(8,128)(2,1)} %param.24) | copy-start | bytes 393220
  172.6 5.6 %collective-permute-start.1 = (bf16[1,512]{1,0:T(2,128)(2,1)S(1)}, bf16[1,512]{1,0:T(2,128)(2,1)S(1)}, u32[]{:S(2)}, u32[]{:S(2)}) collective-permute-start(bf16[1,512]{1,0:T(2,128)(2,1)S(1)} %get-tuple-element.14), channel_id=1, source_target_pairs={{4,0},{8,4},{12,8},{16,12},{20,16},{24,20},{28,24},{5,1},{9,5},{13... | collective-permute-start | bytes 3080 | tf_op jit(solution)/shard_map/ppermute | solution.py:15
Sparse Core Ops, SparseCore 0:
  36.1 21.5 all-gather.2
  59.3 22.5 all-gather.4
  93.1 31.1 reduce-scatter.2
  159.6 67.1 reduce-scatter.4
where the time goes:
time: 236 us; the launch traced here: 235 us
  waiting for transfers between devices  110 us (47%)
  blocking collectives  46.1 us (20%)
  matrix products  33.7 us (14%)
  between operations  14.1 us (6%)
  local copies, waits for them, and re-layouts  10.8 us (5%)
  starting transfers between devices  10.6 us (4%)
  other arithmetic  9.28 us (4%)
    reduce_scatter x1, waiting for transfers between devices, local(): lax.psum_scatter(lax.dot_general(full_h, mixed, (((0,), (0,)), ((), ())),...  47 us
    reduce_scatter x1, waiting for transfers between devices, local(): lax.psum_scatter(partial_value.astype(jnp.bfloat16), 'tp', scatter_dimens...  31.3 us
    all_to_all x1, blocking collectives, local(): lax.all_to_all(send_x, 'sp', split_axis=0, concat_axis=0, tiled=True)  21.7 us
    all_to_all x1, blocking collectives, local(): lax.all_to_all(send_dy, 'sp', split_axis=0, concat_axis=0, tiled=True)  17.6 us
    all_gather x1, waiting for transfers between devices, local(): lax.all_gather(part_dy, 'tp', axis=2, tiled=True)  16.8 us
    all_to_all x1, waiting for transfers between devices, local(): lax.all_to_all(summed.reshape(n_experts, capacity, local_cols), 'sp', spl...  14.3 us
    all_gather x1, blocking collectives, local(): full_h = lax.all_gather(grad_h, 'tp', axis=1, tiled=True)  6.72 us
    all_to_all x1, starting transfers between devices, local(): lax.all_to_all(summed.reshape(n_experts, capacity, local_cols), 'sp', spl...  5.51 us
  transfers between devices with their start and end apart: 7, of which 5 were waited for; matrix products, arithmetic and copies ran while one was open for 11% of the time, Pallas kernels for 0%

commit v1 on v0

v1 whole, which is shorter than its diff:
```python
import functools

import jax
import jax.numpy as jnp
from jax import lax
from jax.experimental import pallas as pl
from jax.experimental.pallas import tpu as pltpu
from jax.sharding import PartitionSpec as P

MESH = pl.DeviceIdType.MESH


def place(n, q):
    s, t = lax.axis_index("sp"), lax.axis_index("tp")
    sibling = t + 1 - 2 * lax.rem(t, 2)
    return s, t, sibling


def greet(n, q):
    s, t, sibling = place(n, q)
    barrier = pltpu.get_barrier_semaphore()
    for i in range(1, n):
        pl.semaphore_signal(
            barrier, inc=1, device_id=(lax.rem(s + i, n), t), device_id_type=MESH
        )
    for d in range(1, q // 2):
        pl.semaphore_signal(
            barrier, inc=1, device_id=(s, lax.rem(t + 2 * d, q)), device_id_type=MESH
        )
    pl.semaphore_signal(barrier, inc=1, device_id=(s, sibling), device_id_type=MESH)
    return barrier, n - 1 + q // 2


def remote(src, dst, send_sem, recv_sem, device):
    return pltpu.make_async_remote_copy(
        src_ref=src,
        dst_ref=dst,
        send_sem=send_sem,
        recv_sem=recv_sem,
        device_id=device,
        device_id_type=MESH,
    )


def dispatch_kernel(
    n, q, ids_ref, w_ref, x_ref, g_ref, xo_ref, do_ref, p_ref,
    p01, send, buf, out_sem, s1, r1, sy, ry, ss, rs,
):
    s, t, sibling = place(n, q)
    ny = q // 2
    tok, cols = x_ref.shape
    total = send.shape[1]
    cap = total // n
    barrier, greeted = greet(n, q)

    ids0, ids1 = ids_ref[0:1, :], ids_ref[1:2, :]
    experts = lax.broadcasted_iota(jnp.int32, (n, tok), 0)
    named = jnp.logical_or(ids0 == experts, ids1 == experts)
    named_f = jnp.where(named, 1.0, 0.0)
    earlier = jnp.where(
        lax.broadcasted_iota(jnp.int32, (tok, tok), 0)
        < lax.broadcasted_iota(jnp.int32, (tok, tok), 1),
        1.0,
        0.0,
    )
    before = jnp.dot(
        named_f.astype(jnp.bfloat16),
        earlier.astype(jnp.bfloat16),
        preferred_element_type=jnp.float32,
    ).astype(jnp.int32)
    slots = lax.broadcasted_iota(jnp.int32, (cap, tok), 0)
    for e in range(n):
        here = before[e : e + 1, :] == slots
        c0 = jnp.where(jnp.logical_and(here, ids0 == e), 1.0, 0.0)
        c1 = jnp.where(jnp.logical_and(here, ids1 == e), 1.0, 0.0)
        rows = slice(e * cap, (e + 1) * cap)
        p01[rows, 0:tok] = c0.astype(jnp.bfloat16)
        p01[rows, tok : 2 * tok] = c1.astype(jnp.bfloat16)
        p_ref[rows, :] = (c0 + c1).astype(jnp.bfloat16)
    grad = g_ref[...].astype(jnp.float32)
    weighted = jnp.concatenate(
        [
            (w_ref[:, 0:1] * grad).astype(jnp.bfloat16),
            (w_ref[:, 1:2] * grad).astype(jnp.bfloat16),
        ],
        axis=0,
    )
    send[0] = jnp.dot(p_ref[...], x_ref[...], preferred_element_type=jnp.float32).astype(
        jnp.bfloat16
    )
    send[1] = jnp.dot(p01[...], weighted, preferred_element_type=jnp.float32).astype(jnp.bfloat16)

    def at_rows(j):
        return pl.ds(pl.multiple_of(j * cap, cap), cap)

    def block(j, tt):
        return buf.at[:, at_rows(j), pl.ds(pl.multiple_of(tt * cols, cols), cols)]

    def first(i):
        e = lax.rem(s + i, n)
        return remote(send.at[:, at_rows(e)], block(s, t), s1.at[i], r1.at[i], (e, t))

    def across(i, d):
        j = lax.rem(s - i + n, n)
        b = block(j, t)
        return remote(b, b, sy.at[i, d - 1], ry.at[i, d - 1], (s, lax.rem(t + 2 * d, q)))

    def beside(i, d):
        j = lax.rem(s - i + n, n)
        b = block(j, lax.rem(t - 2 * d + q, q))
        return remote(b, b, ss.at[i, d], rs.at[i, d], (s, sibling))

    pl.semaphore_wait(barrier, greeted)
    own = pltpu.make_async_copy(send.at[:, at_rows(s)], block(s, t), s1.at[0])
    own.start()
    for i in range(1, n):
        first(i).start()

    def forward(i):
        for d in range(1, ny):
            across(i, d).wait_recv()
            beside(i, d).start()

    outs = []

    def drain(i):
        j = lax.rem(s - i + n, n)
        for d in range(ny):
            beside(i, d).wait_recv()
        for a, ref in enumerate((xo_ref, do_ref)):
            copy = pltpu.make_async_copy(
                buf.at[a, at_rows(j)], ref.at[at_rows(j)], out_sem.at[i, a]
            )
            copy.start()
            outs.append(copy)

    for i in range(n):
        if i == 0:
            own.wait()
        else:
            first(i).wait_recv()
        for d in range(1, ny):
            across(i, d).start()
        beside(i, 0).start()
        if i >= 1:
            forward(i - 1)
        if i >= 2:
            drain(i - 2)
    forward(n - 1)
    for i in range(max(n - 2, 0), n):
        drain(i)
    for i in range(n):
        if i:
            first(i).wait_send()
        for d in range(1, ny):
            across(i, d).wait_send()
        for d in range(ny):
            beside(i, d).wait_send()
    for copy in outs:
        copy.wait()


def dispatch(n, q, ids_t, weight, x, g):
    tok, cols = x.shape
    total = 4 * tok
    ny = q // 2
    vmem = pl.BlockSpec(memory_space=pltpu.VMEM)
    hbm = pl.BlockSpec(memory_space=pl.ANY)
    dma = pltpu.SemaphoreType.DMA
    rows = jax.ShapeDtypeStruct((total, q * cols), jnp.bfloat16)
    return pl.pallas_call(
        functools.partial(dispatch_kernel, n, q),
        out_shape=(rows, rows, jax.ShapeDtypeStruct((total, tok), jnp.bfloat16)),
        in_specs=[vmem] * 4,
        out_specs=(hbm, hbm, vmem),
        scratch_shapes=[
            pltpu.VMEM((total, 2 * tok), jnp.bfloat16),
            pltpu.VMEM((2, total, cols), jnp.bfloat16),
            pltpu.VMEM((2, total, q * cols), jnp.bfloat16),
            dma((n, 2)),
            dma((n,)),
            dma((n,)),
            dma((n, max(ny - 1, 1))),
            dma((n, max(ny - 1, 1))),
            dma((n, ny)),
            dma((n, ny)),
        ],
        compiler_params=pltpu.CompilerParams(collective_id=0, has_side_effects=True),
        name="dispatch",
    )(ids_t, weight, x, g)


def combine_kernel(
    n, q, part_ref, p_ref, g_ref, h_ref,
    rsib, pair, ryb, fin, ret, ss, rs, sy, ry, s3, r3,
):
    s, t, sibling = place(n, q)
    ny = q // 2
    tok, cols = g_ref.shape
    total = part_ref.shape[0]
    cap = total // n
    barrier, greeted = greet(n, q)

    def at_rows(j):
        return pl.ds(pl.multiple_of(j * cap, cap), cap)

    def at_cols(tt):
        return pl.ds(pl.multiple_of(tt * cols, cols), cols)

    def beside(i, d):
        j = lax.rem(s + i, n)
        theirs = lax.rem(sibling + 2 * d, q)
        return remote(
            part_ref.at[at_rows(j), at_cols(theirs)],
            rsib.at[d, at_rows(j)],
            ss.at[i, d],
            rs.at[i, d],
            (s, sibling),
        )

    def across(i, d):
        j = lax.rem(s + i, n)
        return remote(
            pair.at[d - 1, at_rows(j)],
            ryb.at[d - 1, at_rows(j)],
            sy.at[i, d - 1],
            ry.at[i, d - 1],
            (s, lax.rem(t + 2 * d, q)),
        )

    def back(i):
        j = lax.rem(s + i, n)
        return remote(fin.at[at_rows(j)], ret.at[at_rows(s)], s3.at[i], r3.at[i], (j, t))

    def mine(j, d):
        value = part_ref[at_rows(j), at_cols(lax.rem(t + 2 * d, q))].astype(jnp.float32)
        return value + rsib[d, at_rows(j), :].astype(jnp.float32)

    order = [i % n for i in range(1, n + 1)]
    pl.semaphore_wait(barrier, greeted)
    for i in order:
        for d in [*range(1, ny), 0]:
            beside(i, d).start()

    def finish(i):
        j = lax.rem(s + i, n)
        beside(i, 0).wait_recv()
        value = mine(j, 0)
        for d in range(1, ny):
            across(i, d).wait_recv()
            value = value + ryb[d - 1, at_rows(j), :].astype(jnp.float32)
        value = value.astype(jnp.bfloat16)
        if i == 0:
            ret[at_rows(s), :] = value
        else:
            fin[at_rows(j), :] = value
            back(i).start()

    for k, i in enumerate(order):
        j = lax.rem(s + i, n)
        for d in range(1, ny):
            beside(i, d).wait_recv()
            pair[d - 1, at_rows(j), :] = mine(j, d).astype(jnp.bfloat16)
            across(i, d).start()
        if k >= 1:
            finish(order[k - 1])
    finish(order[-1])
    for i in range(1, n):
        back(i).wait_recv()
    moe = lax.dot_general(
        p_ref[...], ret[...], (((0,), (0,)), ((), ())), preferred_element_type=jnp.float32
    )
    h_ref[...] = (g_ref[...].astype(jnp.float32) + moe).astype(jnp.bfloat16)
    for i in range(n):
        if i:
            back(i).wait_send()
        for d in range(1, ny):
            across(i, d).wait_send()
        for d in range(ny):
            beside(i, d).wait_send()


def combine(n, q, part, p, g):
    total = part.shape[0]
    cols = g.shape[1]
    ny = q // 2
    far = max(ny - 1, 1)
    vmem = pl.BlockSpec(memory_space=pltpu.VMEM)
    dma = pltpu.SemaphoreType.DMA
    return pl.pallas_call(
        functools.partial(combine_kernel, n, q),
        out_shape=jax.ShapeDtypeStruct(g.shape, jnp.bfloat16),
        in_specs=[vmem] * 3,
        out_specs=vmem,
        scratch_shapes=[
            pltpu.VMEM((ny, total, cols), jnp.bfloat16),
            pltpu.VMEM((far, total, cols), jnp.bfloat16),
            pltpu.VMEM((far, total, cols), jnp.bfloat16),
            pltpu.VMEM((total, cols), jnp.bfloat16),
            pltpu.VMEM((total, cols), jnp.bfloat16),
            dma((n, ny)),
            dma((n, ny)),
            dma((n, far)),
            dma((n, far)),
            dma((n,)),
            dma((n,)),
        ],
        compiler_params=pltpu.CompilerParams(collective_id=1, has_side_effects=True),
        name="combine",
    )(part, p, g)


def with_halo(block, sides, width):
    for axis, dim in sides:
        count = lax.axis_size(axis)
        forward = [(i, i + 1) for i in range(count - 1)]
        backward = [(target, source) for source, target in forward]
        low = lax.ppermute(
            lax.slice_in_dim(block, block.shape[dim] - width, None, axis=dim), axis, forward
        )
        high = lax.ppermute(lax.slice_in_dim(block, 0, width, axis=dim), axis, backward)
        block = jnp.concatenate([low, block, high], axis=dim)
    return block


def local(
    out_grad,
    moe_input,
    route_weight,
    route_ids,
    gate_proj,
    up_proj,
    down_proj,
    out_proj,
    conv_out,
    gate_b,
    gate_c,
    value_v,
    conv_taps,
):
    n = lax.axis_size("sp")
    q = lax.axis_size("tp")
    tok_rows = out_grad.shape[0]
    mixed = (gate_b.astype(jnp.float32) * conv_out.astype(jnp.float32)).astype(jnp.bfloat16)
    xin, dyin, slots = dispatch(n, q, route_ids.T, route_weight, moe_input, out_grad)
    w_gate = gate_proj[0]
    w_up = up_proj[0]
    w_down = down_proj[0]
    gate = jnp.dot(xin, w_gate, preferred_element_type=jnp.float32)
    upval = jnp.dot(xin, w_up, preferred_element_type=jnp.float32)
    sig = jax.nn.sigmoid(gate)
    act = gate * sig
    hidden = (act * upval).astype(jnp.bfloat16)
    dhid = jnp.dot(dyin, w_down.T, preferred_element_type=jnp.float32)
    dgate = (dhid * upval * (sig * (1.0 + gate * (1.0 - sig)))).astype(jnp.bfloat16)
    dup = (dhid * act).astype(jnp.bfloat16)
    partial_value = jnp.dot(dgate, w_gate.T, preferred_element_type=jnp.float32) + jnp.dot(
        dup, w_up.T, preferred_element_type=jnp.float32
    )
    grad_h = combine(n, q, partial_value.astype(jnp.bfloat16), slots, out_grad)
    grad_down = jnp.dot(hidden.T, dyin, preferred_element_type=jnp.float32).astype(jnp.bfloat16)
    grad_gate = jnp.dot(xin.T, dgate, preferred_element_type=jnp.float32).astype(jnp.bfloat16)
    grad_up = jnp.dot(xin.T, dup, preferred_element_type=jnp.float32).astype(jnp.bfloat16)
    full_h = lax.all_gather(grad_h, "tp", axis=1, tiled=True)
    width = full_h.shape[1]
    all_mixed = lax.all_gather(mixed, "sp", axis=0, tiled=True)
    sent_h = full_h.reshape(tok_rows, n, width // n).transpose(1, 0, 2)
    all_h = lax.all_to_all(sent_h, "sp", split_axis=0, concat_axis=0, tiled=True)
    grad_z = jnp.dot(full_h, out_proj, preferred_element_type=jnp.float32)
    dconv = (grad_z * gate_b.astype(jnp.float32)).astype(jnp.bfloat16)
    grad_b = (grad_z * conv_out.astype(jnp.float32)).astype(jnp.bfloat16)
    padded = with_halo(dconv, (("sp", 0),), 1).astype(jnp.float32)
    grad_u = conv_taps[0] * padded[2:] + conv_taps[1] * padded[1:-1] + conv_taps[2] * padded[:-2]
    grad_c = (grad_u * value_v.astype(jnp.float32)).astype(jnp.bfloat16)
    grad_v = (grad_u * gate_c.astype(jnp.float32)).astype(jnp.bfloat16)
    grad_out = lax.dot_general(
        all_h.reshape(n * tok_rows, width // n),
        all_mixed,
        (((0,), (0,)), ((), ())),
        preferred_element_type=jnp.float32,
    )
    return (grad_gate[None], grad_up[None], grad_down[None], grad_out, grad_b, grad_c, grad_v)


def solution(mesh):
    in_specs = (
        P("sp", "tp"),
        P("sp", "tp"),
        P("sp", None),
        P("sp", None),
        P("sp", None, "tp"),
        P("sp", None, "tp"),
        P("sp", "tp", None),
        P(None, "tp"),
        P("sp", "tp"),
        P("sp", "tp"),
        P("sp", "tp"),
        P("sp", "tp"),
        P(None, "tp"),
    )
    out_specs = (
        P("sp", None, "tp"),
        P("sp", None, "tp"),
        P("sp", "tp", None),
        P("sp", "tp"),
        P("sp", "tp"),
        P("sp", "tp"),
        P("sp", "tp"),
    )
    return jax.shard_map(local, mesh=mesh, in_specs=in_specs, out_specs=out_specs, check_vma=False)
```

time: 236 us -> 162 us (0.69)
  waiting for transfers between devices: 110 us -> 24 us
  Pallas kernels: 0 us -> 70.3 us
  blocking collectives: 46.1 us -> 7.44 us
  other arithmetic: 9.28 us -> 1.49 us
  local copies, waits for them, and re-layouts: 10.8 us -> 4.25 us
  matrix products: 33.7 us -> 29.5 us
    reduce_scatter x2 -> x0, waiting for transfers between devices: 78.4 us -> none  [the longest x1 47 us: local(): lax.psum_scatter(lax.dot_general(full_h, mixed, (((0,), (0,)), ((), ())),...]
    pallas_call x0 -> x2, Pallas kernels: none -> 70.3 us  [the longest x1 40.6 us: dispatch(): pl.pallas_call(functools.partial(dispatch_kernel, n, q), out_shape=(rows,...]
    all_to_all x2 -> x0, blocking collectives: 39.3 us -> none  [the longest x1 21.7 us: local(): lax.all_to_all(send_x, 'sp', split_axis=0, concat_axis=0, tiled=True)]
    all_to_all x1, waiting for transfers between devices: 14.3 us -> 5.24 us  [local(): lax.all_to_all(sent_h, 'sp', split_axis=0, concat_axis=0, tiled=True)]
    dot_general x1, matrix products: 5.37 us -> 2.12 us  [local(): dhid = jnp.dot(dyin, w_down.T, preferred_element_type=jnp.float32)]
    convert_element_type x3 -> x0, other arithmetic: 2.82 us -> none  [the longest x1 1.8 us: local(): grad_out = lax.psum_scatter(lax.dot_general(full_h, mixed, (((0,), (0,)),...]
    all_gather x2 -> x1, waiting for transfers between devices: 16.8 us -> 18.7 us  [local(): all_mixed = lax.all_gather(mixed, 'sp', axis=0, tiled=True)]
  transfers between devices with their start and end apart: 7 -> 4, of which waited for: 5 -> 2; matrix products, arithmetic and copies ran while one was open for 11% -> 9% of each run, Pallas kernels for 0% -> 0%
where the time goes in v1:
time: 162 us
  Pallas kernels  70.3 us (43%)
  matrix products  29.5 us (18%)
  waiting for transfers between devices  24 us (15%)
  between operations  14.3 us (9%)
  starting transfers between devices  10.4 us (6%)
  blocking collectives  7.44 us (5%)
  local copies, waits for them, and re-layouts  4.25 us (3%)
    pallas_call x1, Pallas kernels, dispatch(): pl.pallas_call(functools.partial(dispatch_kernel, n, q), out_shape=(rows,...  40.6 us
    pallas_call x1, Pallas kernels, combine(): pl.pallas_call(functools.partial(combine_kernel, n, q), out_shape=jax.Sha...  29.7 us
    all_gather x1, waiting for transfers between devices, local(): all_mixed = lax.all_gather(mixed, 'sp', axis=0, tiled=True)  18.7 us
    all_gather x1, blocking collectives, local(): full_h = lax.all_gather(grad_h, 'tp', axis=1, tiled=True)  7.44 us
    all_to_all x1, starting transfers between devices, local(): lax.all_to_all(sent_h, 'sp', split_axis=0, concat_axis=0, tiled=True)  6.61 us
    dot_general x1, matrix products, local(): jnp.dot(xin.T, dup, preferred_element_type=jnp.float32).astype(jnp.bfloat16)  5.26 us
    all_to_all x1, waiting for transfers between devices, local(): lax.all_to_all(sent_h, 'sp', split_axis=0, concat_axis=0, tiled=True)  5.24 us
    dot_general x1, matrix products, local(): gate = jnp.dot(xin, w_gate, preferred_element_type=jnp.float32)  3.42 us
  transfers between devices with their start and end apart: 4, of which 2 were waited for; matrix products, arithmetic and copies ran while one was open for 9% of the time, Pallas kernels for 0%

profile of v1, /device:TPU:0, one launch (start us, length us, event | category | flops | bytes accessed | tf_op | source)
XLA Modules:
  0.0 161.6 jit_solution(7122635448345643727)
XLA Ops:
  7.2 0.0 copy-start
  7.2 0.0 all-gather.2.cloned.1.call-start
  7.2 1.6 copy.21.w_ref
  8.8 40.6 %dispatch.1 = (bf16[512,2048]{1,0:T(8,128)(2,1)}, bf16[512,2048]{1,0:T(8,128)(2,1)}, bf16[512,128]{1,0:T(8,128)(2,1)}) custom-call(s32[2,128]{1,0:T(2,128)} %bitcast.53, f32[128,2]{1,0:T(8,128)} %copy.21.w_ref, bf16[128,512]{1,0:T(8,128)(2,1)} %x_ref.1, bf16[128,512]{1,0:T(8,128)(2,1)} %g_ref.3), custom_call_target="tpu_custom_call" | custom-call | tf_op jit(solution)/shard_map/dispatch/pallas_call | solution.py:171
  49.4 0.0 copy-done
  49.4 0.0 copy-start.7
  49.4 0.0 copy-start.8
  49.4 3.4 %fusion.5 = f32[512,704]{0,1:T(8,128)S(1)} fusion(bf16[512,2048]{1,0:T(8,128)(2,1)} %get-tuple-element.10, bf16[1,2048,704]{1,2,0:T(8,128)(2,1)S(1)} %copy-done), kind=kOutput, calls=%fused_computation.9 | convolution fusion | flops 1476395008 | bytes 6422528 | tf_op jit(solution)/shard_map/dot_general | solution.py:349
  52.8 0.0 copy-done.7
  52.9 0.0 copy-done.8
  52.9 0.0 copy-start.13
  52.9 0.0 copy-start.6
  52.9 0.0 copy-start.10
  52.9 1.7 %fusion.8 = f32[512,704]{0,1:T(8,128)S(1)} fusion(bf16[512,2048]{1,0:T(8,128)(2,1)S(1)} %copy-done.8, bf16[1,2048,704]{1,2,0:T(8,128)(2,1)S(1)} %copy-done.7), kind=kOutput, calls=%fused_computation.12 | convolution fusion | flops 1476395008 | bytes 6422528 | tf_op jit(solution)/shard_map/dot_general | solution.py:350
  54.6 0.0 copy-start.15
  54.6 0.0 copy-done.13
  54.6 0.6 copy-done.6
  55.2 1.2 copy-done.10
  56.4 2.1 %multiply_convert_fusion.1 = (bf16[512,704]{0,1:T(8,128)(2,1)S(1)}, bf16[512,704]{0,1:T(8,128)(2,1)S(1)}) fusion(f32[512,704]{0,1:T(8,128)S(1)} %fusion.5, f32[512,704]{0,1:T(8,128)S(1)} %fusion.8, bf16[512,2048]{1,0:T(8,128)(2,1)S(1)} %copy-done.10, bf16[1,704,2048]{2,1,0:T(8,128)(2,1)S(1)} %copy-done.6), kind=kOutput, calls=%fused_computation.17 | convolution fusion | flops 1481080832 | bytes 9306112 | tf_op jit(solution)/shard_map/dot_general | solution.py:354
  58.5 0.0 copy-done.15
  58.5 0.0 copy-start.1
  58.5 0.0 copy-start.12
  58.5 1.9 %fusion.3 = f32[512,2048]{1,0:T(8,128)S(1)} fusion(bf16[512,704]{0,1:T(8,128)(2,1)S(1)} %get-tuple-element.16, bf16[1,2048,704]{1,2,0:T(8,128)(2,1)S(1)} %copy-done), kind=kOutput, calls=%fused_computation.7 | convolution fusion | flops 1476395008 | bytes 7798784 | tf_op jit(solution)/shard_map/dot_general | solution.py:357
  60.4 0.0 copy-done.1
  60.4 0.0 copy-done.12
  60.4 3.3 %add_convert_fusion.part_ref = bf16[512,2048]{1,0:T(8,128)(2,1)} fusion(f32[512,2048]{1,0:T(8,128)S(1)} %fusion.3, bf16[512,704]{0,1:T(8,128)(2,1)S(1)} %get-tuple-element.15, bf16[1,2048,704]{1,2,0:T(8,128)(2,1)S(1)} %copy-done.7), kind=kOutput, calls=%fused_computation | convolution fusion | flops 1478492160 | bytes 9895936 | tf_op jit(solution)/shard_map/dot_general | solution.py:357
  63.8 29.7 %combine.1 = bf16[128,512]{1,0:T(8,128)(2,1)} custom-call(bf16[512,2048]{1,0:T(8,128)(2,1)} %add_convert_fusion.part_ref, bf16[512,128]{1,0:T(8,128)(2,1)} %get-tuple-element.12.p_ref, bf16[128,512]{1,0:T(8,128)(2,1)} %g_ref.3), custom_call_target="tpu_custom_call" | custom-call | tf_op jit(solution)/shard_map/combine/pallas_call | solution.py:290
  93.4 7.4 %all_gather.6 = bf16[128,2048]{1,0:T(8,128)(2,1)S(1)} all-gather(bf16[128,512]{1,0:T(8,128)(2,1)} %combine.1), channel_id=1, replica_groups=mesh['sp'=8,'tp'=4] {'tp'}, dimensions={1}, use_global_device_ids=true | all-gather | bytes 655360 | tf_op jit(solution)/shard_map/all_gather | solution.py:364
  100.9 2.8 %fusion.13 = (bf16[128,512]{1,0:T(8,128)(2,1)S(1)}, bf16[128,512]{1,0:T(8,128)(2,1)}, bf16[128,512]{1,0:T(8,128)(2,1)}) fusion(bf16[128,512]{1,0:T(8,128)(2,1)} %param.22, bf16[128,512]{1,0:T(8,128)(2,1)} %param.21, bf16[128,2048]{1,0:T(8,128)(2,1)S(1)} %all_gather.6, bf16[2048,512]{1,0:T(8,128)(2,1)} %param.20), kind=kOutput, calls=%fused_computation.25 | convolution fusion | flops 268959744 | bytes 3276800 | tf_op jit(solution)/shard_map/dot_general | solution.py:369
  103.7 2.5 %collective-permute-start = (bf16[1,512]{1,0:T(2,128)(2,1)S(1)}, bf16[1,512]{1,0:T(2,128)(2,1)S(1)}, u32[]{:S(2)}, u32[]{:S(2)}) collective-permute-start(bf16[1,512]{1,0:T(2,128)(2,1)S(1)} %get-tuple-element.20), channel_id=1, source_target_pairs={{0,4},{4,8},{8,12},{12,16},{16,20},{20,24},{24,28},{1,5},{5,9},{9,... | collective-permute-start | bytes 3080 | tf_op jit(solution)/shard_map/ppermute | solution.py:318
  106.2 1.3 collective-permute-start.1
  107.5 0.0 all-gather.2.cloned.1.call-update
  107.5 0.8 copy.25
  108.3 6.6 %all-to-all-start = ((bf16[8,128,256]{2,1,0:T(8,128)(2,1)}), bf16[8,128,256]{2,1,0:T(8,128)(2,1)S(1)}, u32[]{:S(2)}, u32[]{:S(2)}) async-start(bf16[8,128,256]{2,1,0:T(8,128)(2,1)} %bitcast.48), calls=%async_computation | async-start | bytes 1048576 | tf_op jit(solution)/shard_map/all_to_all | solution.py:368
  114.9 0.0 copy-start.11
  114.9 0.0 copy-start.14
  114.9 0.0 copy-start.16
  115.0 5.3 %fusion.2 = bf16[1,2048,704]{1,2,0:T(8,128)(2,1)} fusion(bf16[512,704]{0,1:T(8,128)(2,1)} %copy-done.12, bf16[512,2048]{1,0:T(8,128)(2,1)} %get-tuple-element.10), kind=kOutput, calls=%fused_computation.6 | convolution fusion | flops 1477836800 | bytes 5701632 | tf_op jit(solution)/shard_map/dot_general | solution.py:363
  120.2 0.0 copy-done.11
  120.2 0.0 copy-done.14
  120.2 0.0 copy-done.16
  120.2 0.0 copy-start.2
  120.2 0.0 copy-start.9
  120.2 3.3 %fusion = bf16[1,704,2048]{2,1,0:T(8,128)(2,1)} fusion(bf16[512,2048]{1,0:T(8,128)(2,1)S(1)} %copy-done.11, f32[512,704]{0,1:T(8,128)S(1)} %copy-done.16, f32[512,704]{0,1:T(8,128)S(1)} %copy-done.14), kind=kOutput, calls=%fused_computation.4 | convolution fusion | flops 1479999488 | bytes 7864320 | tf_op jit(solution)/shard_map/dot_general | solution.py:361
  123.5 0.0 copy-done.2
  123.5 0.0 copy-done.9
  123.5 0.0 copy-start.5
  123.5 0.0 copy-start.3
  123.6 0.0 copy-start.4
  123.6 3.2 %fusion.1 = bf16[1,2048,704]{1,2,0:T(8,128)(2,1)} fusion(bf16[512,704]{0,1:T(8,128)(2,1)S(1)} %copy-done.2, bf16[512,2048]{1,0:T(8,128)(2,1)S(1)} %copy-done.9), kind=kOutput, calls=%fused_computation.5 | convolution fusion | flops 1477836800 | bytes 5701632 | tf_op jit(solution)/shard_map/dot_general | solution.py:362
  126.8 0.0 copy-done.5
  126.8 0.0 collective-permute-done
  126.8 0.0 collective-permute-done.1
  126.9 0.0 copy-done.3
  126.9 0.8 multiply_convert_fusion.4
  127.7 0.0 copy-done.4
  127.7 0.7 multiply_convert_fusion.5
  128.3 5.2 %all-to-all-done = bf16[8,128,256]{2,1,0:T(8,128)(2,1)S(1)} async-done(((bf16[8,128,256]{2,1,0:T(8,128)(2,1)}), bf16[8,128,256]{2,1,0:T(8,128)(2,1)S(1)}, u32[]{:S(2)}, u32[]{:S(2)}) %all-to-all-start) | async-done | bytes 524320 | tf_op jit(solution)/shard_map/all_to_all | solution.py:368
  133.6 18.7 %all-gather.2.cloned.1.call-done = bf16[1024,512]{1,0:T(8,128)(2,1)} async-done(((bf16[128,512]{1,0:T(8,128)(2,1)}), bf16[1024,512]{1,0:T(8,128)(2,1)}) %all-gather.2.cloned.1.call-update) | async-done | bytes 1048592 | tf_op jit(solution)/shard_map/all_gather | solution.py:366
  152.3 2.5 %fusion.23 = f32[256,512]{1,0:T(8,128)} fusion(bf16[1024,256]{1,0:T(8,128)(2,1)S(1)} %bitcast.49, bf16[1024,512]{1,0:T(8,128)(2,1)} %all-gather.2.cloned.1.call-done), kind=kOutput, calls=%fused_computation.39 | convolution fusion | flops 268435456 | bytes 2097152 | tf_op jit(solution)/shard_map/dot_general | solution.py:376
  (3 shorter events, 0.0 us)
Async XLA Ops:
  7.2 42.2 %copy-start = (bf16[1,2048,704]{1,2,0:T(8,128)(2,1)S(1)}, bf16[1,2048,704]{1,2,0:T(8,128)(2,1)}, u32[]{:S(2)}) copy-start(bf16[1,2048,704]{1,2,0:T(8,128)(2,1)} %param.17) | copy-start | bytes 8650756
  7.2 145.1 %all-gather.2.cloned.1.call-start = ((), (), s32[]{:S(2)}) async-start(), calls=%async_computation.1 | async-start | bytes 1179648 | tf_op jit(solution)/shard_map/all_gather | solution.py:366
  49.4 3.5 %copy-start.7 = (bf16[1,2048,704]{1,2,0:T(8,128)(2,1)S(1)}, bf16[1,2048,704]{1,2,0:T(8,128)(2,1)}, u32[]{:S(2)}) copy-start(bf16[1,2048,704]{1,2,0:T(8,128)(2,1)} %param.18) | copy-start | bytes 8650756
  49.4 3.5 %copy-start.8 = (bf16[512,2048]{1,0:T(8,128)(2,1)S(1)}, bf16[512,2048]{1,0:T(8,128)(2,1)}, u32[]{:S(2)}) copy-start(bf16[512,2048]{1,0:T(8,128)(2,1)} %get-tuple-element.10) | copy-start | bytes 6291460
  52.9 1.7 %copy-start.13 = (f32[512,704]{0,1:T(8,128)}, f32[512,704]{0,1:T(8,128)S(1)}, u32[]{:S(2)}) copy-start(f32[512,704]{0,1:T(8,128)S(1)} %fusion.5) | copy-start | bytes 4325380
  52.9 2.3 %copy-start.6 = (bf16[1,704,2048]{2,1,0:T(8,128)(2,1)S(1)}, bf16[1,704,2048]{2,1,0:T(8,128)(2,1)}, u32[]{:S(2)}) copy-start(bf16[1,704,2048]{2,1,0:T(8,128)(2,1)} %param.19) | copy-start | bytes 8650756
  52.9 3.5 %copy-start.10 = (bf16[512,2048]{1,0:T(8,128)(2,1)S(1)}, bf16[512,2048]{1,0:T(8,128)(2,1)}, u32[]{:S(2)}) copy-start(bf16[512,2048]{1,0:T(8,128)(2,1)} %get-tuple-element.11) | copy-start | bytes 6291460
  54.6 3.9 %copy-start.15 = (f32[512,704]{0,1:T(8,128)}, f32[512,704]{0,1:T(8,128)S(1)}, u32[]{:S(2)}) copy-start(f32[512,704]{0,1:T(8,128)S(1)} %fusion.8) | copy-start | bytes 4325380
  58.5 1.9 %copy-start.1 = (bf16[512,704]{0,1:T(8,128)(2,1)}, bf16[512,704]{0,1:T(8,128)(2,1)S(1)}, u32[]{:S(2)}) copy-start(bf16[512,704]{0,1:T(8,128)(2,1)S(1)} %get-tuple-element.16) | copy-start | bytes 2162692
  58.5 1.9 %copy-start.12 = (bf16[512,704]{0,1:T(8,128)(2,1)}, bf16[512,704]{0,1:T(8,128)(2,1)S(1)}, u32[]{:S(2)}) copy-start(bf16[512,704]{0,1:T(8,128)(2,1)S(1)} %get-tuple-element.15) | copy-start | bytes 2162692
  103.7 23.1 %collective-permute-start = (bf16[1,512]{1,0:T(2,128)(2,1)S(1)}, bf16[1,512]{1,0:T(2,128)(2,1)S(1)}, u32[]{:S(2)}, u32[]{:S(2)}) collective-permute-start(bf16[1,512]{1,0:T(2,128)(2,1)S(1)} %get-tuple-element.20), channel_id=1, source_target_pairs={{0,4},{4,8},{8,12},{12,16},{16,20},{20,24},{24,28},{1,5},{5,9},{9,... | collective-permute-start | bytes 3080 | tf_op jit(solution)/shard_map/ppermute | solution.py:318
  106.2 20.7 %collective-permute-start.1 = (bf16[1,512]{1,0:T(2,128)(2,1)S(1)}, bf16[1,512]{1,0:T(2,128)(2,1)S(1)}, u32[]{:S(2)}, u32[]{:S(2)}) collective-permute-start(bf16[1,512]{1,0:T(2,128)(2,1)S(1)} %get-tuple-element.21), channel_id=1, source_target_pairs={{4,0},{8,4},{12,8},{16,12},{20,16},{24,20},{28,24},{5,1},{9,5},{13... | collective-permute-start | bytes 3080 | tf_op jit(solution)/shard_map/ppermute | solution.py:321
  108.3 25.3 %all-to-all-start = ((bf16[8,128,256]{2,1,0:T(8,128)(2,1)}), bf16[8,128,256]{2,1,0:T(8,128)(2,1)S(1)}, u32[]{:S(2)}, u32[]{:S(2)}) async-start(bf16[8,128,256]{2,1,0:T(8,128)(2,1)} %bitcast.48), calls=%async_computation | async-start | bytes 1048576 | tf_op jit(solution)/shard_map/all_to_all | solution.py:368
  114.9 5.3 %copy-start.11 = (bf16[512,2048]{1,0:T(8,128)(2,1)S(1)}, bf16[512,2048]{1,0:T(8,128)(2,1)}, u32[]{:S(2)}) copy-start(bf16[512,2048]{1,0:T(8,128)(2,1)} %get-tuple-element.11) | copy-start | bytes 6291460
  114.9 5.3 %copy-start.14 = (f32[512,704]{0,1:T(8,128)S(1)}, f32[512,704]{0,1:T(8,128)}, u32[]{:S(2)}) copy-start(f32[512,704]{0,1:T(8,128)} %copy-done.13) | copy-start | bytes 4325380
  114.9 5.3 %copy-start.16 = (f32[512,704]{0,1:T(8,128)S(1)}, f32[512,704]{0,1:T(8,128)}, u32[]{:S(2)}) copy-start(f32[512,704]{0,1:T(8,128)} %copy-done.15) | copy-start | bytes 4325380
  120.2 3.3 %copy-start.2 = (bf16[512,704]{0,1:T(8,128)(2,1)S(1)}, bf16[512,704]{0,1:T(8,128)(2,1)}, u32[]{:S(2)}) copy-start(bf16[512,704]{0,1:T(8,128)(2,1)} %copy-done.1) | copy-start | bytes 2162692
  120.2 3.3 %copy-start.9 = (bf16[512,2048]{1,0:T(8,128)(2,1)S(1)}, bf16[512,2048]{1,0:T(8,128)(2,1)}, u32[]{:S(2)}) copy-start(bf16[512,2048]{1,0:T(8,128)(2,1)} %get-tuple-element.10) | copy-start | bytes 6291460
  123.5 3.3 %copy-start.5 = (f32[3,512]{1,0:T(4,128)S(1)}, f32[3,512]{1,0:T(4,128)}, u32[]{:S(2)}) copy-start(f32[3,512]{1,0:T(4,128)} %param.25) | copy-start | bytes 18436
  123.5 3.3 %copy-start.3 = (bf16[128,512]{1,0:T(8,128)(2,1)S(1)}, bf16[128,512]{1,0:T(8,128)(2,1)}, u32[]{:S(2)}) copy-start(bf16[128,512]{1,0:T(8,128)(2,1)} %param.23) | copy-start | bytes 393220
  123.6 4.1 %copy-start.4 = (bf16[128,512]{1,0:T(8,128)(2,1)S(1)}, bf16[128,512]{1,0:T(8,128)(2,1)}, u32[]{:S(2)}) copy-start(bf16[128,512]{1,0:T(8,128)(2,1)} %param.24) | copy-start | bytes 393220
Sparse Core Ops, SparseCore 0:
  107.6 44.6 all-gather.1

commit v2 on v1

--- a/solution.py
+++ b/solution.py
@@ -191,15 +191,24 @@
 
 
 def combine_kernel(
-    n, q, part_ref, p_ref, g_ref, h_ref,
-    rsib, pair, ryb, fin, ret, ss, rs, sy, ry, s3, r3,
+    n, q, part_ref, p_ref, g_ref, b_ref, co_ref, c_ref, v_ref, taps_ref, w_hbm,
+    gout_ref, gb_ref, gc_ref, gv_ref,
+    rsib, pair, ryb, fin, ret, full_h, h_t, all_t, all_m, w_ref, edge, got, padded, w_sem,
+    ss, rs, sy, ry, s3, r3, sm, rm, sp, rp, shy, rhy, shs, rhs, sa, ra, se, re,
 ):
     s, t, sibling = place(n, q)
+    partner = s + 1 - 2 * lax.rem(s, 2)
     ny = q // 2
     tok, cols = g_ref.shape
-    total = part_ref.shape[0]
+    total, width = part_ref.shape
     cap = total // n
+    share = width // n
     barrier, greeted = greet(n, q)
+    w_copy = pltpu.make_async_copy(w_hbm, w_ref, w_sem)
+    w_copy.start()
+    all_m[s] = (b_ref[...].astype(jnp.float32) * co_ref[...].astype(jnp.float32)).astype(
+        jnp.bfloat16
+    )
 
     def at_rows(j):
         return pl.ds(pl.multiple_of(j * cap, cap), cap)
@@ -232,6 +241,34 @@
         j = lax.rem(s + i, n)
         return remote(fin.at[at_rows(j)], ret.at[at_rows(s)], s3.at[i], r3.at[i], (j, t))
 
+    def mixed_far(i):
+        return remote(
+            all_m.at[s], all_m.at[s], sm.at[i // 2], rm.at[i // 2], (lax.rem(s + i, n), t)
+        )
+
+    def mixed_near(i):
+        b = all_m.at[lax.rem(s - i + n, n)]
+        return remote(b, b, sp.at[i // 2], rp.at[i // 2], (partner, t))
+
+    def h_across(d):
+        b = full_h.at[:, at_cols(t)]
+        return remote(b, b, shy.at[d - 1], rhy.at[d - 1], (s, lax.rem(t + 2 * d, q)))
+
+    def h_beside(d):
+        b = full_h.at[:, at_cols(lax.rem(t - 2 * d + q, q))]
+        return remote(b, b, shs.at[d], rhs.at[d], (s, sibling))
+
+    def h_share(j):
+        return pl.ds(pl.multiple_of(j * share, share), share)
+
+    def h_far(i):
+        j = lax.rem(s + i, n)
+        return remote(h_t.at[h_share(j)], all_t.at[s], sa.at[i], ra.at[i], (j, t))
+
+    def halo(k):
+        there = lax.rem(s + 1, n) if k == 0 else lax.rem(s - 1 + n, n)
+        return remote(edge.at[k], got.at[k], se.at[k], re.at[k], (there, t))
+
     def mine(j, d):
         value = part_ref[at_rows(j), at_cols(lax.rem(t + 2 * d, q))].astype(jnp.float32)
         return value + rsib[d, at_rows(j), :].astype(jnp.float32)
@@ -241,6 +278,9 @@
     for i in order:
         for d in [*range(1, ny), 0]:
             beside(i, d).start()
+    for i in range(2, n, 2):
+        mixed_far(i).start()
+    mixed_near(0).start()
 
     def finish(i):
         j = lax.rem(s + i, n)
@@ -265,62 +305,113 @@
         if k >= 1:
             finish(order[k - 1])
     finish(order[-1])
+    for i in range(2, n, 2):
+        mixed_far(i).wait_recv()
+        mixed_near(i).start()
     for i in range(1, n):
         back(i).wait_recv()
     moe = lax.dot_general(
         p_ref[...], ret[...], (((0,), (0,)), ((), ())), preferred_element_type=jnp.float32
     )
-    h_ref[...] = (g_ref[...].astype(jnp.float32) + moe).astype(jnp.bfloat16)
+    full_h[:, at_cols(t)] = (g_ref[...].astype(jnp.float32) + moe).astype(jnp.bfloat16)
+    for d in range(1, ny):
+        h_across(d).start()
+    h_beside(0).start()
+    w_copy.wait()
+    for d in range(1, ny):
+        h_across(d).wait_recv()
+        h_beside(d).start()
+    for d in range(ny):
+        h_beside(d).wait_recv()
+    for k in range(q):
+        here = slice(k * cols, (k + 1) * cols)
+        h_t[here, :] = full_h[:, here].astype(jnp.float32).T.astype(jnp.bfloat16)
+    for i in range(1, n):
+        h_far(i).start()
+    all_t[s] = h_t[h_share(s), :]
+    grad_z = jnp.dot(full_h[...], w_ref[...], preferred_element_type=jnp.float32)
+    dconv = (grad_z * b_ref[...].astype(jnp.float32)).astype(jnp.bfloat16).astype(jnp.float32)
+    edge[0] = jnp.broadcast_to(dconv[tok - 1 : tok, :], (8, cols))
+    edge[1] = jnp.broadcast_to(dconv[0:1, :], (8, cols))
+    halo(0).start()
+    halo(1).start()
+    gb_ref[...] = (grad_z * co_ref[...].astype(jnp.float32)).astype(jnp.bfloat16)
+    padded[8 : 8 + tok, :] = dconv
+    halo(0).wait_recv()
+    halo(1).wait_recv()
+    padded[0:8, :] = jnp.where(s > 0, got[0], 0.0)
+    padded[8 + tok : 16 + tok, :] = jnp.where(s < n - 1, got[1], 0.0)
+    grad_u = (
+        taps_ref[0:1, :] * padded[9 : 9 + tok, :]
+        + taps_ref[1:2, :] * padded[8 : 8 + tok, :]
+        + taps_ref[2:3, :] * padded[7 : 7 + tok, :]
+    )
+    gc_ref[...] = (grad_u * v_ref[...].astype(jnp.float32)).astype(jnp.bfloat16)
+    gv_ref[...] = (grad_u * c_ref[...].astype(jnp.float32)).astype(jnp.bfloat16)
+    for i in range(0, n, 2):
+        mixed_near(i).wait_recv()
+    for i in range(1, n):
+        h_far(i).wait_recv()
+    total_out = jnp.zeros((share, cols), jnp.float32)
+    for k in range(n):
+        total_out = total_out + jnp.dot(all_t[k], all_m[k], preferred_element_type=jnp.float32)
+    gout_ref[...] = total_out
     for i in range(n):
         if i:
             back(i).wait_send()
+            h_far(i).wait_send()
+        if i % 2 == 0:
+            mixed_near(i).wait_send()
+            if i:
+                mixed_far(i).wait_send()
         for d in range(1, ny):
             across(i, d).wait_send()
         for d in range(ny):
             beside(i, d).wait_send()
-
-
-def combine(n, q, part, p, g):
-    total = part.shape[0]
-    cols = g.shape[1]
+    for d in range(ny):
+        if d:
+            h_across(d).wait_send()
+        h_beside(d).wait_send()
+    halo(0).wait_send()
+    halo(1).wait_send()
+
+
+def combine(n, q, part, p, g, gate_b, conv_out, gate_c, value_v, taps, out_proj):
+    total, width = part.shape
+    tok, cols = g.shape
+    share = width // n
     ny = q // 2
     far = max(ny - 1, 1)
     vmem = pl.BlockSpec(memory_space=pltpu.VMEM)
     dma = pltpu.SemaphoreType.DMA
+    half = jnp.bfloat16
+    like = jax.ShapeDtypeStruct(g.shape, half)
+    sems = [(n, ny), (n, far), (n,), (n // 2,), (n // 2,), (far,), (ny,), (n,), (2,)]
     return pl.pallas_call(
         functools.partial(combine_kernel, n, q),
-        out_shape=jax.ShapeDtypeStruct(g.shape, jnp.bfloat16),
-        in_specs=[vmem] * 3,
-        out_specs=vmem,
+        out_shape=(jax.ShapeDtypeStruct((share, cols), jnp.float32), like, like, like),
+        in_specs=[vmem] * 8 + [pl.BlockSpec(memory_space=pl.ANY)],
+        out_specs=(vmem,) * 4,
         scratch_shapes=[
-            pltpu.VMEM((ny, total, cols), jnp.bfloat16),
-            pltpu.VMEM((far, total, cols), jnp.bfloat16),
-            pltpu.VMEM((far, total, cols), jnp.bfloat16),
-            pltpu.VMEM((total, cols), jnp.bfloat16),
-            pltpu.VMEM((total, cols), jnp.bfloat16),
-            dma((n, ny)),
-            dma((n, ny)),
-            dma((n, far)),
-            dma((n, far)),
-            dma((n,)),
-            dma((n,)),
-        ],
+            pltpu.VMEM((ny, total, cols), half),
+            pltpu.VMEM((far, total, cols), half),
+            pltpu.VMEM((far, total, cols), half),
+            pltpu.VMEM((total, cols), half),
+            pltpu.VMEM((total, cols), half),
+            pltpu.VMEM((tok, width), half),
+            pltpu.VMEM((width, tok), half),
+            pltpu.VMEM((n, share, tok), half),
+            pltpu.VMEM((n, tok, cols), half),
+            pltpu.VMEM(out_proj.shape, half),
+            pltpu.VMEM((2, 8, cols), jnp.float32),
+            pltpu.VMEM((2, 8, cols), jnp.float32),
+            pltpu.VMEM((tok + 16, cols), jnp.float32),
+            dma,
+        ]
+        + [dma(shape) for shape in sems for _ in range(2)],
         compiler_params=pltpu.CompilerParams(collective_id=1, has_side_effects=True),
         name="combine",
-    )(part, p, g)
-
-
-def with_halo(block, sides, width):
-    for axis, dim in sides:
-        count = lax.axis_size(axis)
-        forward = [(i, i + 1) for i in range(count - 1)]
-        backward = [(target, source) for source, target in forward]
-        low = lax.ppermute(
-            lax.slice_in_dim(block, block.shape[dim] - width, None, axis=dim), axis, forward
-        )
-        high = lax.ppermute(lax.slice_in_dim(block, 0, width, axis=dim), axis, backward)
-        block = jnp.concatenate([low, block, high], axis=dim)
-    return block
+    )(part, p, g, gate_b, conv_out, gate_c, value_v, taps, out_proj)
 
 
 def local(
@@ -340,8 +431,6 @@
 ):
     n = lax.axis_size("sp")
     q = lax.axis_size("tp")
-    tok_rows = out_grad.shape[0]
-    mixed = (gate_b.astype(jnp.float32) * conv_out.astype(jnp.float32)).astype(jnp.bfloat16)
     xin, dyin, slots = dispatch(n, q, route_ids.T, route_weight, moe_input, out_grad)
     w_gate = gate_proj[0]
     w_up = up_proj[0]
@@ -357,28 +446,22 @@
     partial_value = jnp.dot(dgate, w_gate.T, preferred_element_type=jnp.float32) + jnp.dot(
         dup, w_up.T, preferred_element_type=jnp.float32
     )
-    grad_h = combine(n, q, partial_value.astype(jnp.bfloat16), slots, out_grad)
+    grad_out, grad_b, grad_c, grad_v = combine(
+        n,
+        q,
+        partial_value.astype(jnp.bfloat16),
+        slots,
+        out_grad,
+        gate_b,
+        conv_out,
+        gate_c,
+        value_v,
+        conv_taps,
+        out_proj,
+    )
     grad_down = jnp.dot(hidden.T, dyin, preferred_element_type=jnp.float32).astype(jnp.bfloat16)
     grad_gate = jnp.dot(xin.T, dgate, preferred_element_type=jnp.float32).astype(jnp.bfloat16)
     grad_up = jnp.dot(xin.T, dup, preferred_element_type=jnp.float32).astype(jnp.bfloat16)
-    full_h = lax.all_gather(grad_h, "tp", axis=1, tiled=True)
-    width = full_h.shape[1]
-    all_mixed = lax.all_gather(mixed, "sp", axis=0, tiled=True)
-    sent_h = full_h.reshape(tok_rows, n, width // n).transpose(1, 0, 2)
-    all_h = lax.all_to_all(sent_h, "sp", split_axis=0, concat_axis=0, tiled=True)
-    grad_z = jnp.dot(full_h, out_proj, preferred_element_type=jnp.float32)
-    dconv = (grad_z * gate_b.astype(jnp.float32)).astype(jnp.bfloat16)
-    grad_b = (grad_z * conv_out.astype(jnp.float32)).astype(jnp.bfloat16)
-    padded = with_halo(dconv, (("sp", 0),), 1).astype(jnp.float32)
-    grad_u = conv_taps[0] * padded[2:] + conv_taps[1] * padded[1:-1] + conv_taps[2] * padded[:-2]
-    grad_c = (grad_u * value_v.astype(jnp.float32)).astype(jnp.bfloat16)
-    grad_v = (grad_u * gate_c.astype(jnp.float32)).astype(jnp.bfloat16)
-    grad_out = lax.dot_general(
-        all_h.reshape(n * tok_rows, width // n),
-        all_mixed,
-        (((0,), (0,)), ((), ())),
-        preferred_element_type=jnp.float32,
-    )
     return (grad_gate[None], grad_up[None], grad_down[None], grad_out, grad_b, grad_c, grad_v)
 
 

time: 162 us -> 128 us (0.79)
  Pallas kernels: 70.3 us -> 96.4 us
  waiting for transfers between devices: 24 us -> 0 us
  between operations: 14.3 us -> 0.88 us
  starting transfers between devices: 10.4 us -> 0 us
  blocking collectives: 7.44 us -> 0 us
  matrix products: 29.5 us -> 24.4 us
  local copies, waits for them, and re-layouts: 4.25 us -> 6.17 us
    pallas_call x1, Pallas kernels: 29.7 us -> 55.8 us  [combine(): pl.pallas_call(functools.partial(combine_kernel, n, q), out_shape=(jax.Sh...]
    all_gather x1 -> x0, waiting for transfers between devices: 18.7 us -> none  [local(): all_mixed = lax.all_gather(mixed, 'sp', axis=0, tiled=True)]
    all_gather x1 -> x0, blocking collectives: 7.44 us -> none  [local(): full_h = lax.all_gather(grad_h, 'tp', axis=1, tiled=True)]
    all_to_all x1 -> x0, starting transfers between devices: 6.61 us -> none  [local(): lax.all_to_all(sent_h, 'sp', split_axis=0, concat_axis=0, tiled=True)]
    dot_general x2 -> x0, matrix products: 5.26 us -> none  [the longest x1 2.79 us: local(): grad_z = jnp.dot(full_h, out_proj, preferred_element_type=jnp.float32)]
    all_to_all x1 -> x0, waiting for transfers between devices: 5.24 us -> none  [local(): lax.all_to_all(sent_h, 'sp', split_axis=0, concat_axis=0, tiled=True)]
    ppermute x2 -> x0, starting transfers between devices: 3.76 us -> none  [the longest x1 2.47 us: with_halo(): lax.ppermute(lax.slice_in_dim(block, block.shape[dim] - width, None, axis...]
    unnamed x35 -> x41, local copies, waits for them, and re-layouts: 3.41 us -> 6.17 us
  transfers between devices with their start and end apart: 4 -> 0, of which waited for: 2 -> 0; matrix products, arithmetic and copies ran while one was open for 9% -> 0% of each run, Pallas kernels for 0% -> 0%
where the time goes in v2:
time: 128 us
  Pallas kernels  96.4 us (75%)
  matrix products  24.4 us (19%)
  local copies, waits for them, and re-layouts  6.17 us (5%)
    pallas_call x1, Pallas kernels, combine(): pl.pallas_call(functools.partial(combine_kernel, n, q), out_shape=(jax.Sh...  55.8 us
    pallas_call x1, Pallas kernels, dispatch(): pl.pallas_call(functools.partial(dispatch_kernel, n, q), out_shape=(rows,...  40.6 us
    unnamed x41, local copies, waits for them, and re-layouts  6.17 us
    dot_general x1, matrix products, local(): jnp.dot(xin.T, dup, preferred_element_type=jnp.float32).astype(jnp.bfloat16)  5.39 us
    dot_general x1, matrix products, local(): gate = jnp.dot(xin, w_gate, preferred_element_type=jnp.float32)  3.43 us
    dot_general x1, matrix products, local(): jnp.dot(dup, w_up.T, preferred_element_type=jnp.float32)  3.32 us
    dot_general x1, matrix products, local(): jnp.dot(hidden.T, dyin, preferred_element_type=jnp.float32)  3.29 us
    dot_general x1, matrix products, local(): jnp.dot(xin.T, dgate, preferred_element_type=jnp.float32)  3.24 us

profile of v2, /device:TPU:0, one launch (start us, length us, event | category | flops | bytes accessed | tf_op | source)
XLA Modules:
  0.0 127.8 jit_solution(18430413930425041881)
XLA Ops:
  0.6 0.0 copy-start
  0.6 1.6 %copy.20.w_ref = f32[128,2]{1,0:T(8,128)} copy(f32[128,2]{0,1:T(2,128)} %param.15) | data formatting | bytes 2048 | tf_op args[2]
  2.2 40.6 %dispatch.1 = (bf16[512,2048]{1,0:T(8,128)(2,1)}, bf16[512,2048]{1,0:T(8,128)(2,1)}, bf16[512,128]{1,0:T(8,128)(2,1)}) custom-call(s32[2,128]{1,0:T(2,128)} %bitcast.32, f32[128,2]{1,0:T(8,128)} %copy.20.w_ref, bf16[128,512]{1,0:T(8,128)(2,1)} %x_ref.1, bf16[128,512]{1,0:T(8,128)(2,1)} %g_ref.3), custom_call_target="tpu_custom_call" | custom-call | tf_op jit(solution)/shard_map/dispatch/pallas_call | solution.py:171
  42.8 0.0 copy-done
  42.8 0.0 copy-start.8
  42.8 0.0 copy-start.11
  42.8 3.4 %fusion.5 = f32[512,704]{0,1:T(8,128)S(1)} fusion(bf16[512,2048]{1,0:T(8,128)(2,1)} %get-tuple-element.14, bf16[1,2048,704]{1,2,0:T(8,128)(2,1)S(1)} %copy-done), kind=kOutput, calls=%fused_computation.9 | convolution fusion | flops 1476395008 | bytes 6422528 | tf_op jit(solution)/shard_map/dot_general | solution.py:438
  46.3 0.0 copy-done.8
  46.3 0.0 copy-done.11
  46.3 0.0 copy-start.14
  46.3 0.0 copy-start.7
  46.3 0.0 copy-start.9
  46.3 1.7 %fusion.8 = f32[512,704]{0,1:T(8,128)S(1)} fusion(bf16[512,2048]{1,0:T(8,128)(2,1)S(1)} %copy-done.11, bf16[1,2048,704]{1,2,0:T(8,128)(2,1)S(1)} %copy-done.8), kind=kOutput, calls=%fused_computation.12 | convolution fusion | flops 1476395008 | bytes 6422528 | tf_op jit(solution)/shard_map/dot_general | solution.py:439
  48.0 0.0 copy-start.16
  48.0 0.0 copy-done.14
  48.0 0.6 copy-done.7
  48.6 1.2 copy-done.9
  49.8 2.1 %multiply_convert_fusion.1 = (bf16[512,704]{0,1:T(8,128)(2,1)S(1)}, bf16[512,704]{0,1:T(8,128)(2,1)S(1)}) fusion(f32[512,704]{0,1:T(8,128)S(1)} %fusion.5, f32[512,704]{0,1:T(8,128)S(1)} %fusion.8, bf16[512,2048]{1,0:T(8,128)(2,1)S(1)} %copy-done.9, bf16[1,704,2048]{2,1,0:T(8,128)(2,1)S(1)} %copy-done.7), kind=kOutput, calls=%fused_computation.17 | convolution fusion | flops 1481080832 | bytes 9306112 | tf_op jit(solution)/shard_map/dot_general | solution.py:443
  51.9 0.0 copy-done.16
  51.9 0.0 copy-start.1
  51.9 0.0 copy-start.13
  52.0 1.9 %fusion.3 = f32[512,2048]{1,0:T(8,128)S(1)} fusion(bf16[512,704]{0,1:T(8,128)(2,1)S(1)} %get-tuple-element.22, bf16[1,2048,704]{1,2,0:T(8,128)(2,1)S(1)} %copy-done), kind=kOutput, calls=%fused_computation.7 | convolution fusion | flops 1476395008 | bytes 7798784 | tf_op jit(solution)/shard_map/dot_general | solution.py:446
  53.8 0.0 copy-done.1
  53.9 0.0 copy-done.13
  53.9 3.3 %add_convert_fusion.part_ref = bf16[512,2048]{1,0:T(8,128)(2,1)} fusion(f32[512,2048]{1,0:T(8,128)S(1)} %fusion.3, bf16[512,704]{0,1:T(8,128)(2,1)S(1)} %get-tuple-element.21, bf16[1,2048,704]{1,2,0:T(8,128)(2,1)S(1)} %copy-done.8), kind=kOutput, calls=%fused_computation | convolution fusion | flops 1478492160 | bytes 9895936 | tf_op jit(solution)/shard_map/dot_general | solution.py:446
  57.2 55.8 %combine.1 = (f32[256,512]{1,0:T(8,128)}, bf16[128,512]{1,0:T(8,128)(2,1)}, bf16[128,512]{1,0:T(8,128)(2,1)}, bf16[128,512]{1,0:T(8,128)(2,1)}) custom-call(bf16[512,2048]{1,0:T(8,128)(2,1)} %add_convert_fusion.part_ref, bf16[512,128]{1,0:T(8,128)(2,1)} %get-tuple-element.16.p_ref, bf16[128,512]{1,0:T(8,128)(2,1)} %g_ref.3, bf16[128,512]{1,0:T(8,128)(2,1)} %b_ref.1, ...), custom_call_target="tpu_custom_call" | custom-call | tf_op jit(solution)/shard_map/combine/pallas_call | solution.py:390
  113.0 0.0 copy-start.2
  113.0 0.0 copy-start.12
  113.0 5.4 %fusion.2 = bf16[1,2048,704]{1,2,0:T(8,128)(2,1)} fusion(bf16[512,704]{0,1:T(8,128)(2,1)} %copy-done.13, bf16[512,2048]{1,0:T(8,128)(2,1)} %get-tuple-element.14), kind=kOutput, calls=%fused_computation.6 | convolution fusion | flops 1477836800 | bytes 5701632 | tf_op jit(solution)/shard_map/dot_general | solution.py:464
  118.4 0.0 copy-done.2
  118.4 0.0 copy-done.12
  118.4 0.0 copy-start.10
  118.4 0.0 copy-start.15
  118.4 0.0 copy-start.17
  118.4 3.2 %fusion.1 = bf16[1,2048,704]{1,2,0:T(8,128)(2,1)} fusion(bf16[512,704]{0,1:T(8,128)(2,1)S(1)} %copy-done.2, bf16[512,2048]{1,0:T(8,128)(2,1)S(1)} %copy-done.12), kind=kOutput, calls=%fused_computation.5 | convolution fusion | flops 1477836800 | bytes 5701632 | tf_op jit(solution)/shard_map/dot_general | solution.py:463
  121.7 0.0 copy-done.10
  121.7 0.0 copy-done.15
  121.7 0.0 copy-done.17
  121.7 0.0 copy-start.3
  121.7 0.0 copy-start.6
  121.7 0.0 copy-start.5
  121.7 0.0 copy-start.4
  121.7 3.3 %fusion = bf16[1,704,2048]{2,1,0:T(8,128)(2,1)} fusion(bf16[512,2048]{1,0:T(8,128)(2,1)S(1)} %copy-done.10, f32[512,704]{0,1:T(8,128)S(1)} %copy-done.17, f32[512,704]{0,1:T(8,128)S(1)} %copy-done.15), kind=kOutput, calls=%fused_computation.4 | convolution fusion | flops 1479999488 | bytes 7864320 | tf_op jit(solution)/shard_map/dot_general | solution.py:462
  125.0 0.0 copy-done.3
  125.0 0.8 copy.25
  125.8 0.0 copy-done.6
  125.8 0.7 copy.26
  126.5 0.0 copy-done.5
  126.5 0.7 copy.27
  127.1 0.0 copy-done.4
  127.1 0.7 copy.28
Async XLA Ops:
  0.6 42.2 %copy-start = (bf16[1,2048,704]{1,2,0:T(8,128)(2,1)S(1)}, bf16[1,2048,704]{1,2,0:T(8,128)(2,1)}, u32[]{:S(2)}) copy-start(bf16[1,2048,704]{1,2,0:T(8,128)(2,1)} %param.17) | copy-start | bytes 8650756
  42.8 3.5 %copy-start.8 = (bf16[1,2048,704]{1,2,0:T(8,128)(2,1)S(1)}, bf16[1,2048,704]{1,2,0:T(8,128)(2,1)}, u32[]{:S(2)}) copy-start(bf16[1,2048,704]{1,2,0:T(8,128)(2,1)} %param.18) | copy-start | bytes 8650756
  42.8 3.5 %copy-start.11 = (bf16[512,2048]{1,0:T(8,128)(2,1)S(1)}, bf16[512,2048]{1,0:T(8,128)(2,1)}, u32[]{:S(2)}) copy-start(bf16[512,2048]{1,0:T(8,128)(2,1)} %get-tuple-element.14) | copy-start | bytes 6291460
  46.3 1.7 %copy-start.14 = (f32[512,704]{0,1:T(8,128)}, f32[512,704]{0,1:T(8,128)S(1)}, u32[]{:S(2)}) copy-start(f32[512,704]{0,1:T(8,128)S(1)} %fusion.5) | copy-start | bytes 4325380
  46.3 2.3 %copy-start.7 = (bf16[1,704,2048]{2,1,0:T(8,128)(2,1)S(1)}, bf16[1,704,2048]{2,1,0:T(8,128)(2,1)}, u32[]{:S(2)}) copy-start(bf16[1,704,2048]{2,1,0:T(8,128)(2,1)} %param.19) | copy-start | bytes 8650756
  46.3 3.5 %copy-start.9 = (bf16[512,2048]{1,0:T(8,128)(2,1)S(1)}, bf16[512,2048]{1,0:T(8,128)(2,1)}, u32[]{:S(2)}) copy-start(bf16[512,2048]{1,0:T(8,128)(2,1)} %get-tuple-element.15) | copy-start | bytes 6291460
  48.0 3.9 %copy-start.16 = (f32[512,704]{0,1:T(8,128)}, f32[512,704]{0,1:T(8,128)S(1)}, u32[]{:S(2)}) copy-start(f32[512,704]{0,1:T(8,128)S(1)} %fusion.8) | copy-start | bytes 4325380
  51.9 1.9 %copy-start.1 = (bf16[512,704]{0,1:T(8,128)(2,1)}, bf16[512,704]{0,1:T(8,128)(2,1)S(1)}, u32[]{:S(2)}) copy-start(bf16[512,704]{0,1:T(8,128)(2,1)S(1)} %get-tuple-element.22) | copy-start | bytes 2162692
  51.9 1.9 %copy-start.13 = (bf16[512,704]{0,1:T(8,128)(2,1)}, bf16[512,704]{0,1:T(8,128)(2,1)S(1)}, u32[]{:S(2)}) copy-start(bf16[512,704]{0,1:T(8,128)(2,1)S(1)} %get-tuple-element.21) | copy-start | bytes 2162692
  113.0 5.4 %copy-start.2 = (bf16[512,704]{0,1:T(8,128)(2,1)S(1)}, bf16[512,704]{0,1:T(8,128)(2,1)}, u32[]{:S(2)}) copy-start(bf16[512,704]{0,1:T(8,128)(2,1)} %copy-done.1) | copy-start | bytes 2162692
  113.0 5.4 %copy-start.12 = (bf16[512,2048]{1,0:T(8,128)(2,1)S(1)}, bf16[512,2048]{1,0:T(8,128)(2,1)}, u32[]{:S(2)}) copy-start(bf16[512,2048]{1,0:T(8,128)(2,1)} %get-tuple-element.14) | copy-start | bytes 6291460
  118.4 3.3 %copy-start.10 = (bf16[512,2048]{1,0:T(8,128)(2,1)S(1)}, bf16[512,2048]{1,0:T(8,128)(2,1)}, u32[]{:S(2)}) copy-start(bf16[512,2048]{1,0:T(8,128)(2,1)} %get-tuple-element.15) | copy-start | bytes 6291460
  118.4 3.3 %copy-start.15 = (f32[512,704]{0,1:T(8,128)S(1)}, f32[512,704]{0,1:T(8,128)}, u32[]{:S(2)}) copy-start(f32[512,704]{0,1:T(8,128)} %copy-done.14) | copy-start | bytes 4325380
  118.4 3.3 %copy-start.17 = (f32[512,704]{0,1:T(8,128)S(1)}, f32[512,704]{0,1:T(8,128)}, u32[]{:S(2)}) copy-start(f32[512,704]{0,1:T(8,128)} %copy-done.16) | copy-start | bytes 4325380
  121.7 3.3 %copy-start.3 = (f32[256,512]{1,0:T(8,128)S(1)}, f32[256,512]{1,0:T(8,128)}, u32[]{:S(2)}) copy-start(f32[256,512]{1,0:T(8,128)} %get-tuple-element.33) | copy-start | bytes 1572868
  121.7 4.1 %copy-start.6 = (bf16[128,512]{1,0:T(8,128)(2,1)S(1)}, bf16[128,512]{1,0:T(8,128)(2,1)}, u32[]{:S(2)}) copy-start(bf16[128,512]{1,0:T(8,128)(2,1)} %get-tuple-element.34) | copy-start | bytes 393220
  121.7 4.8 %copy-start.5 = (bf16[128,512]{1,0:T(8,128)(2,1)S(1)}, bf16[128,512]{1,0:T(8,128)(2,1)}, u32[]{:S(2)}) copy-start(bf16[128,512]{1,0:T(8,128)(2,1)} %get-tuple-element.35) | copy-start | bytes 393220
  121.7 5.4 %copy-start.4 = (bf16[128,512]{1,0:T(8,128)(2,1)S(1)}, bf16[128,512]{1,0:T(8,128)(2,1)}, u32[]{:S(2)}) copy-start(bf16[128,512]{1,0:T(8,128)(2,1)} %get-tuple-element.36) | copy-start | bytes 393220

commit v3 on v2

--- a/solution.py
+++ b/solution.py
@@ -192,8 +192,10 @@
 
 def combine_kernel(
     n, q, part_ref, p_ref, g_ref, b_ref, co_ref, c_ref, v_ref, taps_ref, w_hbm,
-    gout_ref, gb_ref, gc_ref, gv_ref,
-    rsib, pair, ryb, fin, ret, full_h, h_t, all_t, all_m, w_ref, edge, got, padded, w_sem,
+    x_hbm, dy_hbm, hid_hbm, dg_hbm, du_hbm,
+    gout_ref, gb_ref, gc_ref, gv_ref, ggate_hbm, gup_hbm, gdown_hbm,
+    rsib, pair, ryb, fin, ret, full_h, h_t, all_t, all_m, w_ref, edge, got, padded,
+    x_v, dy_v, hid_v, dg_v, du_v, ggate_v, gup_v, gdown_v, in_sem, o_sem, w_sem,
     ss, rs, sy, ry, s3, r3, sm, rm, sp, rp, shy, rhy, shs, rhs, sa, ra, se, re,
 ):
     s, t, sibling = place(n, q)
@@ -205,7 +207,15 @@
     share = width // n
     barrier, greeted = greet(n, q)
     w_copy = pltpu.make_async_copy(w_hbm, w_ref, w_sem)
+    loads = [
+        pltpu.make_async_copy(source, target, in_sem.at[k])
+        for k, (source, target) in enumerate(
+            zip((hid_hbm, dy_hbm, x_hbm, dg_hbm, du_hbm), (hid_v, dy_v, x_v, dg_v, du_v))
+        )
+    ]
     w_copy.start()
+    for load in loads:
+        load.start()
     all_m[s] = (b_ref[...].astype(jnp.float32) * co_ref[...].astype(jnp.float32)).astype(
         jnp.bfloat16
     )
@@ -268,6 +278,24 @@
     def halo(k):
         there = lax.rem(s + 1, n) if k == 0 else lax.rem(s - 1 + n, n)
         return remote(edge.at[k], got.at[k], se.at[k], re.at[k], (there, t))
+
+    over_rows = (((0,), (0,)), ((), ()))
+    stores = [
+        pltpu.make_async_copy(source, target, o_sem.at[k])
+        for k, (source, target) in enumerate(
+            zip((gdown_v, ggate_v, gup_v), (gdown_hbm, ggate_hbm, gup_hbm))
+        )
+    ]
+
+    def grad_step(left, right, target):
+        def step(k, _):
+            here = at_cols(k)
+            target[:, here] = lax.dot_general(
+                left[...], right[:, here], over_rows, preferred_element_type=jnp.float32
+            ).astype(jnp.bfloat16)
+            return 0
+
+        return step
 
     def mine(j, d):
         value = part_ref[at_rows(j), at_cols(lax.rem(t + 2 * d, q))].astype(jnp.float32)
@@ -308,6 +336,10 @@
     for i in range(2, n, 2):
         mixed_far(i).wait_recv()
         mixed_near(i).start()
+    for load in loads:
+        load.wait()
+    lax.fori_loop(0, q, grad_step(hid_v, dy_v, gdown_v), 0)
+    stores[0].start()
     for i in range(1, n):
         back(i).wait_recv()
     moe = lax.dot_general(
@@ -348,6 +380,10 @@
     )
     gc_ref[...] = (grad_u * v_ref[...].astype(jnp.float32)).astype(jnp.bfloat16)
     gv_ref[...] = (grad_u * c_ref[...].astype(jnp.float32)).astype(jnp.bfloat16)
+    lax.fori_loop(0, q, grad_step(dg_v, x_v, ggate_v), 0)
+    stores[1].start()
+    lax.fori_loop(0, q, grad_step(du_v, x_v, gup_v), 0)
+    stores[2].start()
     for i in range(0, n, 2):
         mixed_near(i).wait_recv()
     for i in range(1, n):
@@ -374,9 +410,13 @@
         h_beside(d).wait_send()
     halo(0).wait_send()
     halo(1).wait_send()
-
-
-def combine(n, q, part, p, g, gate_b, conv_out, gate_c, value_v, taps, out_proj):
+    for store in stores:
+        store.wait()
+
+
+def combine(
+    n, q, part, p, g, gate_b, conv_out, gate_c, value_v, taps, out_proj, x, dy, hid, dg, du
+):
     total, width = part.shape
     tok, cols = g.shape
     share = width // n
@@ -386,12 +426,23 @@
     dma = pltpu.SemaphoreType.DMA
     half = jnp.bfloat16
     like = jax.ShapeDtypeStruct(g.shape, half)
+    hbm = pl.BlockSpec(memory_space=pl.ANY)
+    units = hid.shape[1]
+    tall = (units, width)
     sems = [(n, ny), (n, far), (n,), (n // 2,), (n // 2,), (far,), (ny,), (n,), (2,)]
     return pl.pallas_call(
         functools.partial(combine_kernel, n, q),
-        out_shape=(jax.ShapeDtypeStruct((share, cols), jnp.float32), like, like, like),
-        in_specs=[vmem] * 8 + [pl.BlockSpec(memory_space=pl.ANY)],
-        out_specs=(vmem,) * 4,
+        out_shape=(
+            jax.ShapeDtypeStruct((share, cols), jnp.float32),
+            like,
+            like,
+            like,
+            jax.ShapeDtypeStruct(tall, half),
+            jax.ShapeDtypeStruct(tall, half),
+            jax.ShapeDtypeStruct(tall, half),
+        ),
+        in_specs=[vmem] * 8 + [hbm] * 6,
+        out_specs=(vmem,) * 4 + (hbm,) * 3,
         scratch_shapes=[
             pltpu.VMEM((ny, total, cols), half),
             pltpu.VMEM((far, total, cols), half),
@@ -406,12 +457,22 @@
             pltpu.VMEM((2, 8, cols), jnp.float32),
             pltpu.VMEM((2, 8, cols), jnp.float32),
             pltpu.VMEM((tok + 16, cols), jnp.float32),
+            pltpu.VMEM((total, width), half),
+            pltpu.VMEM((total, width), half),
+            pltpu.VMEM((total, units), half),
+            pltpu.VMEM((total, units), half),
+            pltpu.VMEM((total, units), half),
+            pltpu.VMEM(tall, half),
+            pltpu.VMEM(tall, half),
+            pltpu.VMEM(tall, half),
+            dma((5,)),
+            dma((3,)),
             dma,
         ]
         + [dma(shape) for shape in sems for _ in range(2)],
-        compiler_params=pltpu.CompilerParams(collective_id=1, has_side_effects=True),
+        compiler_params=pltpu.CompilerParams(collective_id=1, has_side_effects=True, vmem_limit_bytes=30 * 2**20),
         name="combine",
-    )(part, p, g, gate_b, conv_out, gate_c, value_v, taps, out_proj)
+    )(part, p, g, gate_b, conv_out, gate_c, value_v, taps, out_proj, x, dy, hid, dg, du)
 
 
 def local(
@@ -446,7 +507,7 @@
     partial_value = jnp.dot(dgate, w_gate.T, preferred_element_type=jnp.float32) + jnp.dot(
         dup, w_up.T, preferred_element_type=jnp.float32
     )
-    grad_out, grad_b, grad_c, grad_v = combine(
+    grad_out, grad_b, grad_c, grad_v, grad_gate, grad_up, grad_down = combine(
         n,
         q,
         partial_value.astype(jnp.bfloat16),
@@ -458,11 +519,13 @@
         value_v,
         conv_taps,
         out_proj,
-    )
-    grad_down = jnp.dot(hidden.T, dyin, preferred_element_type=jnp.float32).astype(jnp.bfloat16)
-    grad_gate = jnp.dot(xin.T, dgate, preferred_element_type=jnp.float32).astype(jnp.bfloat16)
-    grad_up = jnp.dot(xin.T, dup, preferred_element_type=jnp.float32).astype(jnp.bfloat16)
-    return (grad_gate[None], grad_up[None], grad_down[None], grad_out, grad_b, grad_c, grad_v)
+        xin,
+        dyin,
+        hidden,
+        dgate,
+        dup,
+    )
+    return (grad_gate.T[None], grad_up.T[None], grad_down[None], grad_out, grad_b, grad_c, grad_v)
 
 
 def solution(mesh):

time: 128 us -> 139 us (1.086)
  local copies, waits for them, and re-layouts: 6.17 us -> 19 us
  matrix products: 24.4 us -> 20.3 us
  Pallas kernels: 96.4 us -> 98.8 us
    dot_general x3 -> x0, matrix products: 11.9 us -> none  [the longest x1 5.39 us: local(): jnp.dot(xin.T, dup, preferred_element_type=jnp.float32).astype(jnp.bfloat16)]
    dot_general x0 -> x2, local copies, waits for them, and re-layouts: none -> 5.95 us  [the longest x1 2.97 us: local(): upval = jnp.dot(xin, w_up, preferred_element_type=jnp.float32)]
    dot_general x1, matrix products: 2.13 us -> 6.11 us  [local(): dhid = jnp.dot(dyin, w_down.T, preferred_element_type=jnp.float32)]
    unnamed x41 -> x32, local copies, waits for them, and re-layouts: 6.17 us -> 10.1 us
    dot_general x1, matrix products: 1.69 us -> 5.23 us  [local(): upval = jnp.dot(xin, w_up, preferred_element_type=jnp.float32)]
    mul x0 -> x1, local copies, waits for them, and re-layouts: none -> 2.97 us  [local(): dhid * upval * (sig * (1.0 + gate * (1.0 - sig)))]
    pallas_call x1, Pallas kernels: 55.8 us -> 58.2 us  [combine(): pl.pallas_call(functools.partial(combine_kernel, n, q), out_shape=(jax.Sh...]
    dot_general x1, matrix products: 3.43 us -> 5.31 us  [local(): gate = jnp.dot(xin, w_gate, preferred_element_type=jnp.float32)]
where the time goes in v3:
time: 139 us
  Pallas kernels  98.8 us (71%)
  matrix products  20.3 us (15%)
  local copies, waits for them, and re-layouts  19 us (14%)
    pallas_call x1, Pallas kernels, combine(): pl.pallas_call(functools.partial(combine_kernel, n, q), out_shape=(jax.Sh...  58.2 us
    pallas_call x1, Pallas kernels, dispatch(): pl.pallas_call(functools.partial(dispatch_kernel, n, q), out_shape=(rows,...  40.6 us
    unnamed x32, local copies, waits for them, and re-layouts  10.1 us
    dot_general x1, matrix products, local(): dhid = jnp.dot(dyin, w_down.T, preferred_element_type=jnp.float32)  6.11 us
    dot_general x1, matrix products, local(): gate = jnp.dot(xin, w_gate, preferred_element_type=jnp.float32)  5.31 us
    dot_general x1, matrix products, local(): upval = jnp.dot(xin, w_up, preferred_element_type=jnp.float32)  5.23 us
    dot_general x1, local copies, waits for them, and re-layouts, local(): upval = jnp.dot(xin, w_up, preferred_element_type=jnp.float32)  2.97 us
    dot_general x1, local copies, waits for them, and re-layouts, local(): dhid = jnp.dot(dyin, w_down.T, preferred_element_type=jnp.float32)  2.97 us

profile of v3, /device:TPU:0, one launch (start us, length us, event | category | flops | bytes accessed | tf_op | source)
XLA Modules:
  0.0 138.9 jit_solution(13770827953936937048)
XLA Ops:
  0.6 0.0 copy-start
  0.6 1.6 %copy.28.w_ref = f32[128,2]{1,0:T(8,128)} copy(f32[128,2]{0,1:T(2,128)} %param.15) | data formatting | bytes 2048 | tf_op args[2]
  2.2 40.6 %dispatch.1 = (bf16[512,2048]{1,0:T(8,128)(2,1)}, bf16[512,2048]{1,0:T(8,128)(2,1)}, bf16[512,128]{1,0:T(8,128)(2,1)}) custom-call(s32[2,128]{1,0:T(2,128)} %bitcast.33, f32[128,2]{1,0:T(8,128)} %copy.28.w_ref, bf16[128,512]{1,0:T(8,128)(2,1)} %x_ref.1, bf16[128,512]{1,0:T(8,128)(2,1)} %g_ref.3), custom_call_target="tpu_custom_call" | custom-call | tf_op jit(solution)/shard_map/dispatch/pallas_call | solution.py:171
  42.8 5.2 %fusion.5 = f32[512,704]{0,1:T(8,128)} fusion(bf16[512,2048]{1,0:T(8,128)(2,1)} %get-tuple-element.18.x_hbm, bf16[1,2048,704]{1,2,0:T(8,128)(2,1)} %param.18), kind=kOutput, calls=%fused_computation.6 | convolution fusion | flops 1476395008 | bytes 6422528 | tf_op jit(solution)/shard_map/dot_general | solution.py:500
  48.0 3.0 %copy.34 = f32[512,704]{1,0:T(8,128)} copy(f32[512,704]{0,1:T(8,128)} %fusion.5) | data formatting | bytes 2883584 | tf_op jit(solution)/shard_map/dot_general | solution.py:500
  51.0 6.1 %fusion.10 = (f32[512,704]{0,1:T(8,128)}, f32[512,704]{0,1:T(8,128)}) fusion(f32[512,704]{0,1:T(8,128)} %fusion.5, bf16[512,2048]{1,0:T(8,128)(2,1)} %get-tuple-element.17.dy_hbm, bf16[1,704,2048]{2,1,0:T(8,128)(2,1)} %param.19), kind=kOutput, calls=%fused_computation.15 | convolution fusion | flops 1476755456 | bytes 9306112 | tf_op jit(solution)/shard_map/dot_general | solution.py:504
  57.1 3.0 %copy.31 = f32[512,704]{1,0:T(8,128)} copy(f32[512,704]{0,1:T(8,128)} %get-tuple-element.30) | data formatting | bytes 2883584 | tf_op jit(solution)/shard_map/mul | solution.py:505
  60.1 3.0 %copy.33 = f32[512,704]{1,0:T(8,128)} copy(f32[512,704]{0,1:T(8,128)} %get-tuple-element.31) | data formatting | bytes 2883584 | tf_op jit(solution)/shard_map/dot_general | solution.py:504
  63.1 0.0 copy-done
  63.1 5.3 %multiply_convert_fusion = (bf16[512,704]{1,0:T(8,128)(2,1)S(1)}, bf16[512,704]{1,0:T(8,128)(2,1)S(1)}, bf16[512,704]{1,0:T(8,128)(2,1)S(1)}) fusion(f32[512,704]{1,0:T(8,128)} %copy.34, f32[512,704]{1,0:T(8,128)} %copy.31, f32[512,704]{1,0:T(8,128)} %copy.33, bf16[512,2048]{1,0:T(8,128)(2,1)} %get-tuple-element.18.x_hbm, bf16[1,2048,704]{1,2,0:T(8,128)(2,1)S(1)} %copy-done), kind=kOutput, calls=%fused_computation.10 | convolution fusion | flops 1481441280 | bytes 11468800 | tf_op jit(solution)/shard_map/dot_general | solution.py:499
  68.4 0.0 copy-start.11
  68.4 1.8 %fusion = f32[512,2048]{1,0:T(8,128)S(1)} fusion(bf16[512,704]{1,0:T(8,128)(2,1)S(1)} %get-tuple-element.28.dg_hbm, bf16[1,2048,704]{1,2,0:T(8,128)(2,1)S(1)} %copy-done), kind=kOutput, calls=%fused_computation.1 | convolution fusion | flops 1476395008 | bytes 7798784 | tf_op jit(solution)/shard_map/dot_general | solution.py:507
  70.2 0.0 copy-done.11
  70.2 0.0 copy-start.1
  70.2 0.0 copy-start.2
  70.2 0.0 copy-start.3
  70.2 0.0 copy-start.4
  70.3 0.0 copy-start.5
  70.3 0.0 copy-start.6
  70.3 0.0 copy-start.7
  70.3 0.0 copy-start.8
  70.3 0.0 copy-start.9
  70.3 0.0 copy-start.10
  70.3 1.8 %add_convert_fusion.part_ref = bf16[512,2048]{1,0:T(8,128)(2,1)S(1)} fusion(f32[512,2048]{1,0:T(8,128)S(1)} %fusion, bf16[512,704]{1,0:T(8,128)(2,1)S(1)} %get-tuple-element.29.du_hbm, bf16[1,2048,704]{1,2,0:T(8,128)(2,1)S(1)} %copy-done.11), kind=kOutput, calls=%fused_computation | convolution fusion | flops 1478492160 | bytes 9895936 | tf_op jit(solution)/shard_map/dot_general | solution.py:507
  72.2 0.0 copy-done.1
  72.2 0.3 copy-done.2
  72.4 0.6 copy-done.3
  73.1 0.0 copy-done.4
  73.1 0.0 copy-done.5
  73.1 0.0 copy-done.6
  73.1 0.0 copy-done.7
  73.1 0.0 copy-done.8
  73.1 0.0 copy-done.9
  73.2 0.0 copy-done.10
  73.2 58.2 %combine.1 = (f32[256,512]{1,0:T(8,128)S(1)}, bf16[128,512]{1,0:T(8,128)(2,1)S(1)}, bf16[128,512]{1,0:T(8,128)(2,1)S(1)}, bf16[128,512]{1,0:T(8,128)(2,1)S(1)}, ...) custom-call(bf16[512,2048]{1,0:T(8,128)(2,1)S(1)} %add_convert_fusion.part_ref, ...), custom_call_target="tpu_custom_call" | custom-call | tf_op jit(solution)/shard_map/combine/pallas_call | solution.py:433
  131.4 1.6 %copy.43 = bf16[1,2048,704]{1,2,0:T(8,128)(2,1)} copy(bf16[1,2048,704]{1,2,0:T(8,128)(2,1)S(1)} %bitcast.32) | data formatting | bytes 5767168
  133.0 1.6 %copy.44 = bf16[1,2048,704]{1,2,0:T(8,128)(2,1)} copy(bf16[1,2048,704]{1,2,0:T(8,128)(2,1)S(1)} %bitcast.31) | data formatting | bytes 5767168
  134.5 1.6 %copy.45 = bf16[1,704,2048]{2,1,0:T(8,128)(2,1)} copy(bf16[1,704,2048]{2,1,0:T(8,128)(2,1)S(1)} %bitcast.30) | data formatting | bytes 5767168
  136.1 0.8 copy.46
  136.9 0.7 copy.47
  137.6 0.7 copy.48
  138.2 0.7 copy.49
Async XLA Ops:
  0.6 62.4 %copy-start = (bf16[1,2048,704]{1,2,0:T(8,128)(2,1)S(1)}, bf16[1,2048,704]{1,2,0:T(8,128)(2,1)}, u32[]{:S(2)}) copy-start(bf16[1,2048,704]{1,2,0:T(8,128)(2,1)} %param.17) | copy-start | bytes 8650756
  68.4 1.8 %copy-start.11 = (bf16[1,2048,704]{1,2,0:T(8,128)(2,1)S(1)}, bf16[1,2048,704]{1,2,0:T(8,128)(2,1)}, u32[]{:S(2)}) copy-start(bf16[1,2048,704]{1,2,0:T(8,128)(2,1)} %param.18) | copy-start | bytes 8650756
  70.2 2.0 %copy-start.1 = (bf16[2048,512]{1,0:T(8,128)(2,1)S(1)}, bf16[2048,512]{1,0:T(8,128)(2,1)}, u32[]{:S(2)}) copy-start(bf16[2048,512]{1,0:T(8,128)(2,1)} %w_hbm.1) | copy-start | bytes 6291460
  70.2 2.2 %copy-start.2 = (bf16[512,2048]{1,0:T(8,128)(2,1)S(1)}, bf16[512,2048]{1,0:T(8,128)(2,1)}, u32[]{:S(2)}) copy-start(bf16[512,2048]{1,0:T(8,128)(2,1)} %get-tuple-element.18.x_hbm) | copy-start | bytes 6291460
  70.2 2.8 %copy-start.3 = (bf16[512,2048]{1,0:T(8,128)(2,1)S(1)}, bf16[512,2048]{1,0:T(8,128)(2,1)}, u32[]{:S(2)}) copy-start(bf16[512,2048]{1,0:T(8,128)(2,1)} %get-tuple-element.17.dy_hbm) | copy-start | bytes 6291460
  70.2 2.8 %copy-start.4 = (bf16[128,512]{1,0:T(8,128)(2,1)S(1)}, bf16[128,512]{1,0:T(8,128)(2,1)}, u32[]{:S(2)}) copy-start(bf16[128,512]{1,0:T(8,128)(2,1)} %g_ref.3) | copy-start | bytes 393220
  70.3 2.8 %copy-start.5 = (bf16[128,512]{1,0:T(8,128)(2,1)S(1)}, bf16[128,512]{1,0:T(8,128)(2,1)}, u32[]{:S(2)}) copy-start(bf16[128,512]{1,0:T(8,128)(2,1)} %b_ref.1) | copy-start | bytes 393220
  70.3 2.8 %copy-start.6 = (bf16[128,512]{1,0:T(8,128)(2,1)S(1)}, bf16[128,512]{1,0:T(8,128)(2,1)}, u32[]{:S(2)}) copy-start(bf16[128,512]{1,0:T(8,128)(2,1)} %co_ref.1) | copy-start | bytes 393220
  70.3 2.8 %copy-start.7 = (bf16[128,512]{1,0:T(8,128)(2,1)S(1)}, bf16[128,512]{1,0:T(8,128)(2,1)}, u32[]{:S(2)}) copy-start(bf16[128,512]{1,0:T(8,128)(2,1)} %c_ref.1) | copy-start | bytes 393220
  70.3 2.8 %copy-start.8 = (bf16[128,512]{1,0:T(8,128)(2,1)S(1)}, bf16[128,512]{1,0:T(8,128)(2,1)}, u32[]{:S(2)}) copy-start(bf16[128,512]{1,0:T(8,128)(2,1)} %v_ref.1) | copy-start | bytes 393220
  70.3 2.9 %copy-start.9 = (bf16[512,128]{1,0:T(8,128)(2,1)S(1)}, bf16[512,128]{1,0:T(8,128)(2,1)}, u32[]{:S(2)}) copy-start(bf16[512,128]{1,0:T(8,128)(2,1)} %get-tuple-element.19.p_ref) | copy-start | bytes 393220
  70.3 2.9 %copy-start.10 = (f32[3,512]{1,0:T(4,128)S(1)}, f32[3,512]{1,0:T(4,128)}, u32[]{:S(2)}) copy-start(f32[3,512]{1,0:T(4,128)} %taps_ref.1) | copy-start | bytes 18436
